TPU v7x, 256 devices: a 4x2x16 block of a 4x16x16 slice. The times are simulated.
256 devices in a mesh: grp: 2 (over y), sp: 32 (over z, core), tp: 4 (over x).
Axes of the slice: x: 4, y: 2, z: 16, core: 2. Of those that a mesh axis runs over, the one named last changes fastest.
The devices are a block of a 4x16x16 slice.
Arguments:
- query_rows: bfloat16 [32768, 1024], P(('grp', 'sp'), 'tp'), parts along dimension 0, may hold values from -128 to 128
- key_rows: bfloat16 [32768, 256], P(('grp', 'sp'), 'tp'), parts along dimension 0, may hold values from -4 to 4
- value_rows: bfloat16 [32768, 256], P(('grp', 'sp'), 'tp'), parts along dimension 0, may hold values from -6 to 6
- sink_logits: float32 [16], P('tp'), may hold values from 3 to 7
- residual: bfloat16 [32768, 2048], P(('grp', 'sp', 'tp')), parts along dimension 0, may hold values from -6 to 6
- out_weight: bfloat16 [1024, 2048], P('tp'), may hold values from -0.1875 to 0.1875
- norm_gain: float32 [2048], replicated, may hold values from 0.1 to 1.9
- gate_weight: bfloat16 [128, 2048, 512], P(('sp', 'tp')), may hold values from -0.125 to 0.125
- up_weight: bfloat16 [128, 2048, 512], P(('sp', 'tp')), may hold values from -0.125 to 0.125
- down_weight: bfloat16 [128, 512, 2048], P(('sp', 'tp')), may hold values from -0.25 to 0.25
- routes: int32 [32768, 2], P(('grp', 'sp', 'tp')), parts along dimension 0, may hold values from 0 to 127, as said below
- route_weight: float32 [32768, 2], P(('grp', 'sp', 'tp')), parts along dimension 0, may hold values from 0.1 to 1
Outputs:
- layer_out: bfloat16 [32768, 2048], P(('grp', 'sp', 'tp')), parts along dimension 0
There are 2 independent parts, one for each index of `grp`. A program takes and returns all parts, laid end to end along the dimension named above; an argument that names none is the same for every part. Nothing has to cross between parts.
Inputs may be any that keep to these rules, and one draw needn't show every extreme that they name: `routes`: A token's two experts differ and lie in the same group of 32 consecutive experts. Among the 128 tokens of one device (aligned blocks of 128 rows) no expert is named more than 4 times; in every block each expert of one group, the same group for all blocks, is named exactly 4 times.
All inputs are finite; a program needn't handle non-finite values.
Results may differ from a plain program's by a relative error of at most 0.013.
Values may be sent and summed in bfloat16 or wider, within the bound.
A program may use at most 64 MiB of HBM per device.

v0:
```python
import jax
import jax.numpy as jnp
from jax import lax
from jax.sharding import PartitionSpec as P

HDIM = 64
WINDOW = 128


rope_base = 10000.0
norm_eps = 1e-06


def shifted(block, axis, distance):
    devices = range(lax.axis_size(axis))
    route = [(i - distance, i) for i in devices if i - distance in devices]
    return lax.ppermute(block, axis, route)


def cut_along(x, dim, size):
    lengths = x.shape
    tiles = x.reshape(*lengths[:dim], size, lengths[dim] // size, *lengths[dim + 1 :])
    return jnp.moveaxis(tiles, dim, 0)


def summed_on_arrival(x, axis, dim):
    size = lax.axis_size(axis)
    tiles = lax.all_to_all(cut_along(x, dim, size), axis, 0, 0, tiled=True)
    return jnp.sum(tiles.astype(jnp.float32), axis=0)


def rotate(rows, positions, heads):
    half_dim = HDIM // 2
    values = rows.astype(jnp.float32).reshape(rows.shape[0], heads, HDIM)
    inverse = rope_base ** (-jnp.arange(half_dim, dtype=jnp.float32) / half_dim)
    angles = positions.astype(jnp.float32)[:, None] * inverse[None, :]
    cosines = jnp.cos(angles)[:, None, :]
    sines = jnp.sin(angles)[:, None, :]
    lower = values[..., :half_dim]
    upper = values[..., half_dim:]
    turned = jnp.concatenate(
        [lower * cosines - upper * sines, upper * cosines + lower * sines], axis=-1
    )
    return turned.reshape(rows.shape[0], heads * HDIM).astype(jnp.bfloat16)


def per_device(
    query_rows,
    key_rows,
    value_rows,
    sink_logits,
    residual,
    out_weight,
    norm_gain,
    gate_weight,
    up_weight,
    down_weight,
    routes,
    route_weight,
):
    tok_count = query_rows.shape[0]
    head_local = query_rows.shape[1] // HDIM
    group_local = key_rows.shape[1] // HDIM
    repeat = head_local // group_local
    first_pos = lax.axis_index("sp") * tok_count
    positions = first_pos + jnp.arange(tok_count, dtype=jnp.int32)
    rot_q = rotate(query_rows, positions, head_local)
    rot_k = rotate(key_rows, positions, group_local)
    tails = jnp.stack([rot_k[tok_count - WINDOW :], value_rows[tok_count - WINDOW :]])
    earlier = shifted(tails, "sp", 1)
    blocks = tok_count // WINDOW
    q_blocks = rot_q.reshape(blocks, WINDOW, group_local, repeat, HDIM)
    k_blocks = rot_k.reshape(blocks, WINDOW, group_local, HDIM)
    v_blocks = value_rows.reshape(blocks, WINDOW, group_local, HDIM)
    k_prev = jnp.concatenate(
        [earlier[0].reshape(1, WINDOW, group_local, HDIM), k_blocks[:-1]], axis=0
    )
    v_prev = jnp.concatenate(
        [earlier[1].reshape(1, WINDOW, group_local, HDIM), v_blocks[:-1]], axis=0
    )
    k_wide = jnp.concatenate([k_prev, k_blocks], axis=1)
    v_wide = jnp.concatenate([v_prev, v_blocks], axis=1)
    query_pos = jnp.arange(WINDOW) + WINDOW
    key_pos = jnp.arange(2 * WINDOW)
    distance = query_pos[:, None] - key_pos[None, :]
    in_band = (distance >= 0) & (distance < WINDOW)
    key_global = (
        first_pos + jnp.arange(blocks)[:, None, None] * WINDOW + key_pos[None, None, :] - WINDOW
    )
    allowed = in_band[None] & (key_global >= 0)
    scores = jnp.einsum(
        "nqgrd,nkgd->grnqk", q_blocks, k_wide, preferred_element_type=jnp.float32
    ) * HDIM ** (-0.5)
    scores = jnp.where(allowed[None, None], scores, -jnp.inf)
    sink_here = sink_logits.reshape(group_local, repeat)[:, :, None, None, None]
    largest = jnp.maximum(scores.max(axis=-1, keepdims=True), sink_here)
    exp_scores = jnp.exp(scores - largest)
    denominator = exp_scores.sum(axis=-1, keepdims=True) + jnp.exp(sink_here - largest)
    probs = (exp_scores / denominator).astype(jnp.bfloat16)
    attended = jnp.einsum("grnqk,nkgd->nqgrd", probs, v_wide, preferred_element_type=jnp.float32)
    attended = attended.astype(jnp.bfloat16).reshape(tok_count, head_local * HDIM)
    row_count = residual.shape[0]
    projected = summed_on_arrival(
        jnp.dot(attended, out_weight, preferred_element_type=jnp.float32).astype(jnp.bfloat16),
        "tp",
        0,
    )
    stream_f = (residual.astype(jnp.float32) + projected).astype(jnp.bfloat16).astype(jnp.float32)
    normed = (
        stream_f
        * lax.rsqrt(jnp.mean(stream_f * stream_f, axis=-1, keepdims=True) + norm_eps)
        * norm_gain[None, :]
    ).astype(jnp.bfloat16)
    sp_count = lax.axis_size("sp")
    tp_count = lax.axis_size("tp")
    expert_count = sp_count * tp_count
    capacity = 4 * row_count // expert_count
    width = normed.shape[1]
    flat_expert = routes.reshape(-1)
    one_hot = (flat_expert[:, None] == jnp.arange(expert_count, dtype=jnp.int32)[None, :]).astype(
        jnp.int32
    )
    slot_rank = jnp.sum((jnp.cumsum(one_hot, axis=0) - one_hot) * one_hot, axis=1)
    slot_index = flat_expert * capacity + slot_rank
    token_of = jnp.arange(2 * row_count, dtype=jnp.int32) // 2
    outgoing = (
        jnp.zeros((expert_count * capacity, width), jnp.bfloat16)
        .at[slot_index]
        .set(normed[token_of])
    )
    outgoing = outgoing.reshape(expert_count, capacity, width)
    arrived = lax.all_to_all(outgoing, ("sp", "tp"), split_axis=0, concat_axis=0, tiled=True)
    flat_rows = arrived.reshape(-1, width)
    gate_out = jnp.dot(flat_rows, gate_weight[0], preferred_element_type=jnp.float32)
    up_out = jnp.dot(flat_rows, up_weight[0], preferred_element_type=jnp.float32)
    hidden = (jax.nn.silu(gate_out) * up_out).astype(jnp.bfloat16)
    produced = jnp.dot(hidden, down_weight[0], preferred_element_type=jnp.float32).astype(
        jnp.bfloat16
    )
    returned = lax.all_to_all(
        produced.reshape(arrived.shape), ("sp", "tp"), split_axis=0, concat_axis=0, tiled=True
    )
    gathered = returned.reshape(expert_count * capacity, width)[slot_index].astype(jnp.float32)
    weighted = gathered * route_weight.reshape(-1)[:, None]
    combined = weighted.reshape(row_count, 2, width).sum(axis=1)
    return (stream_f + combined).astype(jnp.bfloat16)


def solution(mesh):
    in_specs = (
        P(("grp", "sp"), "tp"),
        P(("grp", "sp"), "tp"),
        P(("grp", "sp"), "tp"),
        P("tp"),
        P(("grp", "sp", "tp"), None),
        P("tp", None),
        P(),
        P(("sp", "tp"), None, None),
        P(("sp", "tp"), None, None),
        P(("sp", "tp"), None, None),
        P(("grp", "sp", "tp"), None),
        P(("grp", "sp", "tp"), None),
    )
    out_specs = P(("grp", "sp", "tp"), None)
    return jax.shard_map(
        per_device, mesh=mesh, in_specs=in_specs, out_specs=out_specs, check_vma=False
    )
```

profile of v0, /device:TPU:40, one launch (start us, length us, event | category | flops | bytes accessed | tf_op | source)
XLA Modules:
  0.0 328.1 jit_solution(8339543554724609521)
XLA Ops:
  0.0 1.0 bitcast_convert_fusion
  1.0 0.3 fusion.47
  1.4 0.7 slice_bitcast_fusion.4
  2.1 1.8 collective-permute-start
  4.0 0.3 multiply_cosine_fusion
  4.3 1.1 copy.21
  5.4 0.1 convert.12
  5.5 0.1 add_compare_fusion
  5.6 0.2 broadcast_and_fusion
  5.8 0.1 subtract_convert_fusion
  5.9 0.0 copy-start.6
  6.1 0.5 fusion.53
  6.6 0.1 broadcast_maximum_fusion
  6.7 0.3 fusion.5
  7.0 0.1 exponential_add_fusion
  7.1 0.5 fusion.12
  7.6 0.2 copy.24
  7.8 0.5 copy-done.1
  8.3 2.0 convolution_convert_fusion
  10.3 4.7 %all-to-all-start = ((bf16[4,128,2048]{2,1,0:T(8,128)(2,1)}), bf16[4,128,2048]{2,1,0:T(8,128)(2,1)}, u32[]{:S(2)}, u32[]{:S(2)}) async-start(bf16[4,128,2048]{2,1,0:T(8,128)(2,1)} %bitcast.105), calls=%async_computation | async-start | bytes 4194304 | tf_op jit(solution)/shard_map/all_to_all | solution.py:28
  15.0 0.1 copy.26
  15.1 0.1 eq.29
  15.3 0.1 eq.25
  15.4 0.1 copy.28
  15.5 0.2 fusion.28
  15.9 0.1 copy.25
  16.0 0.1 mul.180
  16.1 0.2 fusion.38
  16.3 0.0 copy-start.4
  16.3 24.6 %all-to-all-done = bf16[4,128,2048]{2,1,0:T(8,128)(2,1)} async-done(((bf16[4,128,2048]{2,1,0:T(8,128)(2,1)}), bf16[4,128,2048]{2,1,0:T(8,128)(2,1)}, u32[]{:S(2)}, u32[]{:S(2)}) %all-to-all-start) | async-done | bytes 2097184 | tf_op jit(solution)/shard_map/all_to_all | solution.py:28
  40.9 2.1 convert_reduce_fusion
  43.0 0.3 fusion.13
  43.3 0.2 fusion.15
  43.5 7.0 %scatter_custom_fusion = bf16[512,2048]{1,0:T(8,128)(2,1)} fusion(s32[256]{0:T(256)S(1)} %bitcast.112, bf16[128,2048]{1,0:T(8,128)(2,1)S(1)} %fusion.15, s32[1024]{0:T(1024)S(1)} %pad_clamp_fusion.1, bf16[]{:T(256)} %constant.57.clone.1), kind=kCustom, calls=%fused_computation.28 | custom fusion | bytes 2097154 | tf_op jit(solution)/shard_map/scatter | solution.py:129
  50.5 4.1 %reshape.386 = bf16[128,4,2048]{2,1,0:T(4,128)(2,1)} reshape(bf16[512,2048]{1,0:T(8,128)(2,1)} %scatter_custom_fusion) | data formatting | bytes 4194304 | tf_op jit(solution)/shard_map/reshape | solution.py:131
  54.6 128.5 %all_to_all.15 = bf16[128,4,2048]{2,1,0:T(4,128)(2,1)} all-to-all(bf16[128,4,2048]{2,1,0:T(4,128)(2,1)} %reshape.386), channel_id=1, replica_groups=mesh['grp'=2,'sp'=32,'tp'=4] {'sp','tp'}, dimensions={0} | all-to-all | bytes 4194304 | tf_op jit(solution)/shard_map/all_to_all | solution.py:132
  183.1 4.0 %reshape.387 = bf16[512,2048]{1,0:T(8,128)(2,1)} reshape(bf16[128,4,2048]{2,1,0:T(4,128)(2,1)} %all_to_all.15) | data formatting | bytes 4194304 | tf_op jit(solution)/shard_map/reshape | solution.py:133
  187.1 4.4 %fusion.3 = f32[512,512]{1,0:T(8,128)} fusion(bf16[512,2048]{1,0:T(8,128)(2,1)} %reshape.387, bf16[1,2048,512]{2,1,0:T(8,128)(2,1)} %param.19), kind=kOutput, calls=%fused_computation.10 | convolution fusion | flops 1073741824 | bytes 5242880 | tf_op jit(solution)/shard_map/dot_general | solution.py:134
  191.5 6.2 %convolution_convert_fusion.1 = bf16[512,2048]{1,0:T(8,128)(2,1)} fusion(bf16[1,512,2048]{2,1,0:T(8,128)(2,1)S(1)} %copy-done, bf16[512,2048]{1,0:T(8,128)(2,1)} %reshape.387, bf16[1,2048,512]{2,1,0:T(8,128)(2,1)} %param.20, f32[512,512]{1,0:T(8,128)} %fusion.3), kind=kOutput, calls=%fused_computation.5 | convolution fusion | flops 2150105088 | bytes 9437184 | tf_op jit(solution)/shard_map/dot_general | solution.py:137
  197.8 4.1 %reshape.388 = bf16[128,4,2048]{2,1,0:T(4,128)(2,1)} reshape(bf16[512,2048]{1,0:T(8,128)(2,1)} %convolution_convert_fusion.1) | data formatting | bytes 4194304 | tf_op jit(solution)/shard_map/reshape | solution.py:141
  201.9 12.4 %all-to-all-start.2 = ((bf16[128,4,2048]{2,1,0:T(4,128)(2,1)}), bf16[128,4,2048]{2,1,0:T(4,128)(2,1)}, u32[]{:S(2)}, u32[]{:S(2)}) async-start(bf16[128,4,2048]{2,1,0:T(4,128)(2,1)} %reshape.388), calls=%async_computation.2 | async-start | bytes 4194304 | tf_op jit(solution)/shard_map/all_to_all | solution.py:140
  214.3 0.1 copy.30
  214.4 95.4 %all-to-all-done.2 = bf16[128,4,2048]{2,1,0:T(4,128)(2,1)} async-done(((bf16[128,4,2048]{2,1,0:T(4,128)(2,1)}), bf16[128,4,2048]{2,1,0:T(4,128)(2,1)}, u32[]{:S(2)}, u32[]{:S(2)}) %all-to-all-start.2) | async-done | bytes 2097184 | tf_op jit(solution)/shard_map/all_to_all | solution.py:140
  309.8 4.0 %reshape.389 = bf16[512,2048]{1,0:T(8,128)(2,1)} reshape(bf16[128,4,2048]{2,1,0:T(4,128)(2,1)} %all-to-all-done.2) | data formatting | bytes 4194304 | tf_op jit(solution)/shard_map/reshape | solution.py:143
  313.7 5.2 %gather_fusion = bf16[256,2048]{1,0:T(8,128)(2,1)} fusion(bf16[512,2048]{1,0:T(8,128)(2,1)} %reshape.389, s32[1024]{0:T(1024)S(1)} %pad_clamp_fusion), kind=kCustom, calls=%fused_computation.1 | custom fusion | bytes 2098176 | tf_op jit(solution)/shard_map/gather | solution.py:143
  318.9 3.4 %reshape.394 = f32[128,2,2048]{2,1,0:T(2,128)} reshape(bf16[256,2048]{1,0:T(8,128)(2,1)} %gather_fusion) | data formatting | bytes 3145728 | tf_op jit(solution)/shard_map/convert_element_type | solution.py:143
  322.3 4.8 %multiply_reduce_fusion = f32[128,2048]{1,0:T(8,128)S(1)} fusion(f32[128,2,2048]{2,1,0:T(2,128)} %reshape.394, f32[128,2]{1,0:T(8,128)S(1)} %copy.30), kind=kLoop, calls=%fused_computation.12 | loop fusion | flops 786432 | bytes 3146752 | tf_op jit(solution)/shard_map/reduce_sum | solution.py:145
  327.1 0.9 fusion.16
  (43 shorter events, 0.3 us)
Async XLA Ops:
  0.0 191.5 %copy-start = (bf16[1,512,2048]{2,1,0:T(8,128)(2,1)S(1)}, bf16[1,512,2048]{2,1,0:T(8,128)(2,1)}, u32[]{:S(2)}) copy-start(bf16[1,512,2048]{2,1,0:T(8,128)(2,1)} %param.21) | copy-start | bytes 6291460
  0.0 5.9 %copy-start.3 = (bf16[512,64]{0,1:T(8,128)(2,1)S(1)}, bf16[512,64]{0,1:T(8,128)(2,1)}, u32[]{:S(2)}) copy-start(bf16[512,64]{0,1:T(8,128)(2,1)} %param.14) | copy-start | bytes 196612
  0.0 6.0 %slice-start = ((bf16[512,64]{0,1:T(8,128)(2,1)}), bf16[384,64]{0,1:T(8,128)(2,1)S(1)}, s32[]{:S(2)}) async-start(bf16[512,64]{0,1:T(8,128)(2,1)} %param.14), calls=%async_computation.3 | async-start | bytes 98304 | tf_op jit(solution)/shard_map/slice | solution.py:79
  2.1 3.9 %collective-permute-start = (bf16[2,128,64]{1,2,0:T(8,128)(2,1)S(1)}, bf16[2,128,64]{1,2,0:T(8,128)(2,1)S(1)}, u32[]{:S(2)}, u32[]{:S(2)}) collective-permute-start(bf16[2,128,64]{1,2,0:T(8,128)(2,1)S(1)} %pad_maximum_fusion), channel_id=1, source_target_pairs={{0,4},{4,8},{8,12},{12,16},{16,20},{20,24},{24,28},{28,32},{32,36}... | collective-permute-start | bytes 98312 | tf_op jit(solution)/shard_map/ppermute | solution.py:17
  5.9 0.7 copy-start.6
  7.0 1.2 copy-start.1
  10.3 4.7 %copy-start.5 = (s32[128,2]{0,1:T(2,128)S(1)}, s32[128,2]{0,1:T(2,128)}, u32[]{:S(2)}) copy-start(s32[128,2]{0,1:T(2,128)} %param.22) | copy-start | bytes 3076
  10.3 30.6 %all-to-all-start = ((bf16[4,128,2048]{2,1,0:T(8,128)(2,1)}), bf16[4,128,2048]{2,1,0:T(8,128)(2,1)}, u32[]{:S(2)}, u32[]{:S(2)}) async-start(bf16[4,128,2048]{2,1,0:T(8,128)(2,1)} %bitcast.105), calls=%async_computation | async-start | bytes 4194304 | tf_op jit(solution)/shard_map/all_to_all | solution.py:28
  15.5 27.5 %copy-start.2 = (bf16[128,2048]{1,0:T(8,128)(2,1)S(1)}, bf16[128,2048]{1,0:T(8,128)(2,1)}, u32[]{:S(2)}) copy-start(bf16[128,2048]{1,0:T(8,128)(2,1)} %param.16) | copy-start | bytes 1572868
  16.3 27.0 %copy-start.4 = (f32[2048]{0:T(1024)S(1)}, f32[2048]{0:T(1024)}, u32[]{:S(2)}) copy-start(f32[2048]{0:T(1024)} %param.18) | copy-start | bytes 24580
  201.9 12.4 %copy-start.7 = (f32[128,2]{0,1:T(2,128)S(1)}, f32[128,2]{0,1:T(2,128)}, u32[]{:S(2)}) copy-start(f32[128,2]{0,1:T(2,128)} %param.23) | copy-start | bytes 3076
  201.9 107.9 %all-to-all-start.2 = ((bf16[128,4,2048]{2,1,0:T(4,128)(2,1)}), bf16[128,4,2048]{2,1,0:T(4,128)(2,1)}, u32[]{:S(2)}, u32[]{:S(2)}) async-start(bf16[128,4,2048]{2,1,0:T(4,128)(2,1)} %reshape.388), calls=%async_computation.2 | async-start | bytes 4194304 | tf_op jit(solution)/shard_map/all_to_all | solution.py:140
where the time goes:
time: 330 us; the launch traced here: 328 us
  blocking collectives  129 us (39%)
  waiting for transfers between devices  120 us (36%)
  local copies, waits for them, and re-layouts  35.3 us (11%)
  starting transfers between devices  18.9 us (6%)
  matrix products  13.7 us (4%)
  other arithmetic  11.4 us (3%)
    all_to_all x1, blocking collectives, per_device(): lax.all_to_all(outgoing, ('sp', 'tp'), split_axis=0, concat_axis=0, tiled...  129 us
    all_to_all x1, waiting for transfers between devices, per_device(): lax.all_to_all(produced.reshape(arrived.shape), ('sp', 'tp'), split_axis=...  95.4 us
    all_to_all x1, waiting for transfers between devices, summed_on_arrival(): tiles = lax.all_to_all(cut_along(x, dim, size), axis, 0, 0, tiled=True)  24.6 us
    all_to_all x1, starting transfers between devices, per_device(): lax.all_to_all(produced.reshape(arrived.shape), ('sp', 'tp'), split_axis=...  12.4 us
    scatter x1, local copies, waits for them, and re-layouts, per_device(): outgoing = jnp.zeros((expert_count * capacity, width), jnp.bfloat16).at[s...  7 us
  transfers between devices with their start and end apart: 3, of which 2 were waited for; matrix products, arithmetic and copies ran while one was open for 1% of the time, Pallas kernels for 0%

commit v1 on v0

--- a/solution.py
+++ b/solution.py
@@ -1,7 +1,15 @@
+import functools
+
 import jax
 import jax.numpy as jnp
 from jax import lax
+from jax.experimental import pallas as pl
+from jax.experimental.pallas import tpu as pltpu
 from jax.sharding import PartitionSpec as P
+
+MESH_ID = pl.DeviceIdType.MESH
+CAP = 4
+CORES = 2
 
 HDIM = 64
 WINDOW = 128
@@ -42,6 +50,348 @@
         [lower * cosines - upper * sines, upper * cosines + lower * sines], axis=-1
     )
     return turned.reshape(rows.shape[0], heads * HDIM).astype(jnp.bfloat16)
+
+
+def expert_kernel(
+    ring,
+    xs,
+    tile,
+    normed_ref,
+    stream_ref,
+    meta_ref,
+    gate_hbm,
+    up_hbm,
+    down_hbm,
+    out_ref,
+    pool,
+    pool_meta,
+    picked,
+    routed,
+    made,
+    back,
+    left_sum,
+    right_sum,
+    left_own,
+    right_own,
+    gate_w,
+    up_w,
+    down_w,
+    weight_sem,
+    pool_send,
+    pool_recv,
+    meta_send,
+    meta_recv,
+    pick_send,
+    pick_recv,
+    back_send,
+    back_recv,
+    sum_send,
+    sum_recv,
+):
+    f32, bf16 = jnp.float32, jnp.bfloat16
+    rows, width = normed_ref.shape
+    half = rows // 2
+    far = ring // 2
+    peers = xs * CORES
+    sp, tp = lax.axis_index("sp"), lax.axis_index("tp")
+    core = lax.rem(sp, CORES)
+    z = sp // CORES
+    mine = core * xs + tp
+    nxt = {"sp": lax.rem(sp + CORES, ring * CORES)}
+    prv = {"sp": lax.rem(sp + (ring - 1) * CORES, ring * CORES)}
+
+    def peer(offset):
+        u = lax.rem(mine + offset, peers)
+        return u, {"sp": z * CORES + u // xs, "tp": lax.rem(u, xs)}
+
+    loads = [
+        pltpu.make_async_copy(src, dst, weight_sem.at[i])
+        for i, (src, dst) in enumerate(((gate_hbm, gate_w), (up_hbm, up_w), (down_hbm, down_w)))
+    ]
+    for load in loads:
+        load.start()
+
+    barrier = pltpu.get_barrier_semaphore()
+    pl.semaphore_signal(barrier, inc=1, device_id=nxt, device_id_type=MESH_ID)
+    pl.semaphore_signal(barrier, inc=1, device_id=prv, device_id_type=MESH_ID)
+    for o in range(1, peers):
+        pl.semaphore_signal(barrier, inc=1, device_id=peer(o)[1], device_id_type=MESH_ID)
+    pl.semaphore_wait(barrier, peers + 1)
+
+    def part(h):
+        return pl.ds(h * half, half)
+
+    def send_pool(way, slot, h, src=None):
+        to = slot + 1 if way == 0 else lax.rem(slot + ring - 1, ring)
+        step = slot if way == 0 else lax.rem(ring - slot, ring)
+        src = pool.at[slot, part(h)] if src is None else src
+        return pltpu.make_async_remote_copy(
+            src_ref=src,
+            dst_ref=pool.at[to, part(h)],
+            send_sem=pool_send.at[way, step, h],
+            recv_sem=pool_recv.at[way, step, h],
+            device_id=nxt if way == 0 else prv,
+            device_id_type=MESH_ID,
+        )
+
+    def send_meta(way, slot, src=None):
+        to = slot + 1 if way == 0 else lax.rem(slot + ring - 1, ring)
+        step = slot if way == 0 else lax.rem(ring - slot, ring)
+        return pltpu.make_async_remote_copy(
+            src_ref=pool_meta.at[slot] if src is None else src,
+            dst_ref=pool_meta.at[to],
+            send_sem=meta_send.at[way, step],
+            recv_sem=meta_recv.at[way, step],
+            device_id=nxt if way == 0 else prv,
+            device_id_type=MESH_ID,
+        )
+
+    for way in range(2):
+        send_meta(way, 0, meta_ref).start()
+        for h in range(2):
+            send_pool(way, 0, h, normed_ref.at[part(h)]).start()
+    pool[0] = normed_ref[...]
+    pool_meta[0] = meta_ref[...]
+
+    row_id = lax.broadcasted_iota(jnp.int32, (peers * 2 * CAP, rows), 0)
+    local_code = (row_id // (2 * CAP)) * CAP + lax.rem(row_id, CAP)
+    in_second = lax.rem(row_id, 2 * CAP) >= CAP
+    base = z * (peers * CAP)
+
+    def matches(slot, second):
+        here = jnp.where(in_second == second, local_code + base, -1).astype(f32)
+        m = pool_meta[slot]
+        return here == m[0:1, :], here == m[1:2, :], m
+
+    def pick_of(slot, second):
+        first_hit, second_hit, _ = matches(slot, second)
+        return (first_hit | second_hit).astype(f32).astype(bf16)
+
+    def weights_of(slot, second):
+        first_hit, second_hit, m = matches(slot, second)
+        w = jnp.where(first_hit, m[2:3, :], 0.0) + jnp.where(second_hit, m[3:4, :], 0.0)
+        high = w.astype(bf16)
+        return high, (w - high.astype(f32)).astype(bf16)
+
+    def exchange(src, dst, sends, recvs, step, offset):
+        u, where = peer(offset)
+        return pltpu.make_async_remote_copy(
+            src_ref=src.at[step, u],
+            dst_ref=dst.at[step, mine],
+            send_sem=sends.at[step, offset],
+            recv_sem=recvs.at[step, offset],
+            device_id=where,
+            device_id_type=MESH_ID,
+        )
+
+    def pick(step):
+        a, b = step, ring - 1 - step
+        one_a, one_b = pick_of(a, False), pick_of(b, True)
+        for c in range(width // tile):
+            cols = pl.ds(c * tile, tile)
+            got = jnp.dot(one_a, pool[a, :, cols], preferred_element_type=f32)
+            got += jnp.dot(one_b, pool[b, :, cols], preferred_element_type=f32)
+            got = got.astype(bf16).reshape(peers, 2 * CAP, tile)
+            picked[step, :, :, cols] = got
+        for o in range(1, peers):
+            exchange(picked, routed, pick_send, pick_recv, step, o).start()
+        routed[step, mine] = picked[step, mine]
+
+    def serve(step):
+        for o in range(1, peers):
+            exchange(picked, routed, pick_send, pick_recv, step, o).wait_recv()
+        x = routed[step].reshape(peers * 2 * CAP, width)
+        g = jnp.dot(x, gate_w[...], preferred_element_type=f32)
+        u = jnp.dot(x, up_w[...], preferred_element_type=f32)
+        hidden = (g * (1.0 / (1.0 + jnp.exp(-g))) * u).astype(bf16)
+        for c in range(width // tile):
+            cols = pl.ds(c * tile, tile)
+            y = jnp.dot(hidden, down_w[:, cols], preferred_element_type=f32)
+            made[step, :, :, cols] = y.astype(bf16).reshape(peers, 2 * CAP, tile)
+        for o in range(1, peers):
+            exchange(made, back, back_send, back_recv, step, o).start()
+        back[step, mine] = made[step, mine]
+
+    def ring_step(n, _):
+        for h in range(2):
+            send_pool(0, n - 1, h).wait_recv()
+
+            @pl.when((n < far - 1) | (h == 0))
+            def _():
+                send_pool(0, n, h).start()
+
+            send_pool(1, lax.rem(ring - n + 1, ring), h).wait_recv()
+
+            @pl.when((n < far - 1) | (h == 1))
+            def _():
+                send_pool(1, ring - n, h).start()
+
+            if h == 0:
+                send_meta(0, n - 1).wait_recv()
+                send_meta(0, n).start()
+                send_meta(1, lax.rem(ring - n + 1, ring)).wait_recv()
+
+                @pl.when(n < far - 1)
+                def _():
+                    send_meta(1, ring - n).start()
+
+                @pl.when(n >= 2)
+                def _():
+                    serve(n - 2)
+            else:
+                pick(n - 1)
+        return 0
+
+    for load in loads:
+        load.wait()
+    lax.fori_loop(1, far, ring_step, 0)
+    serve(far - 2)
+    send_meta(0, far - 1).wait_recv()
+    send_pool(0, far - 1, 0).wait_recv()
+    send_pool(1, ring - far + 1, 1).wait_recv()
+    pick(far - 1)
+    serve(far - 1)
+
+    contract = (((0,), (0,)), ((), ()))
+
+    def wait_back(step):
+        for o in range(1, peers):
+            exchange(made, back, back_send, back_recv, step, o).wait_recv()
+
+    def own_share(slot, step, second, dst):
+        high, low = weights_of(slot, second)
+        w = jnp.concatenate([high, low], axis=0)
+        for c in range(width // tile):
+            cols = pl.ds(c * tile, tile)
+            y = back[step, :, :, cols].reshape(peers * 2 * CAP, tile)
+            y = jnp.concatenate([y, y], axis=0)
+            dst[:, cols] = lax.dot_general(w, y, contract, preferred_element_type=f32)
+
+    def send_sum(way, d, h):
+        buf = left_sum if way == 0 else right_sum
+        return pltpu.make_async_remote_copy(
+            src_ref=buf.at[d, part(h)],
+            dst_ref=buf.at[d - 1, part(h)],
+            send_sem=sum_send.at[way, d - 1, h],
+            recv_sem=sum_recv.at[way, d - 1, h],
+            device_id=prv if way == 0 else nxt,
+            device_id_type=MESH_ID,
+        )
+
+    wait_back(far - 1)
+    own_share(far, far - 1, True, left_own)
+    left_sum[far, part(0)] = left_own[part(0)].astype(bf16)
+    send_sum(0, far, 0).start()
+    right_sum[far, part(1)] = left_own[part(1)].astype(bf16)
+    send_sum(1, far, 1).start()
+
+    def sum_step(i, _):
+        d = far - 1 - i
+        wait_back(d - 1)
+        own_share(d, d, False, left_own)
+        own_share(ring - d, d - 1, True, right_own)
+        for way, own, buf, order in ((0, left_own, left_sum, (1, 0)), (1, right_own, right_sum, (0, 1))):
+            h = order[0]
+
+            @pl.when(d < far - 1)
+            def _():
+                send_sum(way, d + 1, h).wait_recv()
+                buf[d, part(h)] = (buf[d, part(h)].astype(f32) + own[part(h)]).astype(bf16)
+
+            @pl.when(d == far - 1)
+            def _():
+                buf[d, part(h)] = own[part(h)].astype(bf16)
+
+            send_sum(way, d, h).start()
+        for way, own, buf, order in ((0, left_own, left_sum, (1, 0)), (1, right_own, right_sum, (0, 1))):
+            h = order[1]
+            send_sum(way, d + 1, h).wait_recv()
+            buf[d, part(h)] = (buf[d, part(h)].astype(f32) + own[part(h)]).astype(bf16)
+            send_sum(way, d, h).start()
+        return 0
+
+    lax.fori_loop(0, far - 1, sum_step, 0)
+    own_share(0, 0, False, left_own)
+    left_own[...] += stream_ref[...].astype(f32)
+    for h in (1, 0):
+        send_sum(0, 1, h).wait_recv()
+        send_sum(1, 1, h).wait_recv()
+        total = left_own[part(h)] + left_sum[0, part(h)].astype(f32)
+        out_ref[part(h)] = (total + right_sum[0, part(h)].astype(f32)).astype(bf16)
+
+    def drain(n, _):
+        for way in range(2):
+            slot = n if way == 0 else lax.rem(ring - n, ring)
+            for h in range(2):
+
+                @pl.when((n < far - 1) | (h == way))
+                def _():
+                    send_pool(way, slot, h).wait_send()
+
+                @pl.when((n < far - 1) | (h == way))
+                def _():
+                    send_sum(way, n + 1, h).wait_send()
+
+            @pl.when((n < far - 1) | (way == 0))
+            def _():
+                send_meta(way, slot).wait_send()
+
+        for o in range(1, peers):
+            exchange(picked, routed, pick_send, pick_recv, n, o).wait_send()
+            exchange(made, back, back_send, back_recv, n, o).wait_send()
+        return 0
+
+    lax.fori_loop(0, far, drain, 0)
+
+
+def routed_experts(normed, stream, meta, gate, up, down):
+    rows, width = normed.shape
+    ring = lax.axis_size("sp") // CORES
+    xs = lax.axis_size("tp")
+    far = ring // 2
+    peers = xs * CORES
+    hidden = gate.shape[1]
+    tile = min(512, width)
+    bf16 = jnp.bfloat16
+    vmem = pl.BlockSpec(memory_space=pltpu.VMEM)
+    hbm = pl.BlockSpec(memory_space=pl.ANY)
+    slab = (far, peers, 2 * CAP, width)
+    dma = pltpu.SemaphoreType.DMA
+    return pl.pallas_call(
+        functools.partial(expert_kernel, ring, xs, tile),
+        out_shape=jax.ShapeDtypeStruct((rows, width), bf16),
+        in_specs=[vmem, vmem, vmem, hbm, hbm, hbm],
+        out_specs=vmem,
+        scratch_shapes=[
+            pltpu.VMEM((ring, rows, width), bf16),
+            pltpu.VMEM((ring, 8, rows), jnp.float32),
+            pltpu.VMEM(slab, bf16),
+            pltpu.VMEM(slab, bf16),
+            pltpu.VMEM(slab, bf16),
+            pltpu.VMEM(slab, bf16),
+            pltpu.VMEM((far + 1, rows, width), bf16),
+            pltpu.VMEM((far + 1, rows, width), bf16),
+            pltpu.VMEM((rows, width), jnp.float32),
+            pltpu.VMEM((rows, width), jnp.float32),
+            pltpu.VMEM((width, hidden), bf16),
+            pltpu.VMEM((width, hidden), bf16),
+            pltpu.VMEM((hidden, width), bf16),
+            dma((3,)),
+            dma((2, far, 2)),
+            dma((2, far, 2)),
+            dma((2, far)),
+            dma((2, far)),
+            dma((far, peers)),
+            dma((far, peers)),
+            dma((far, peers)),
+            dma((far, peers)),
+            dma((2, far, 2)),
+            dma((2, far, 2)),
+        ],
+        compiler_params=pltpu.CompilerParams(
+            collective_id=1, has_side_effects=True, vmem_limit_bytes=60 * 1024 * 1024
+        ),
+    )(normed, stream, meta, gate, up, down)
 
 
 def per_device(
@@ -111,39 +461,20 @@
         * lax.rsqrt(jnp.mean(stream_f * stream_f, axis=-1, keepdims=True) + norm_eps)
         * norm_gain[None, :]
     ).astype(jnp.bfloat16)
-    sp_count = lax.axis_size("sp")
-    tp_count = lax.axis_size("tp")
-    expert_count = sp_count * tp_count
-    capacity = 4 * row_count // expert_count
     width = normed.shape[1]
+    expert_count = lax.axis_size("sp") * lax.axis_size("tp")
     flat_expert = routes.reshape(-1)
     one_hot = (flat_expert[:, None] == jnp.arange(expert_count, dtype=jnp.int32)[None, :]).astype(
         jnp.int32
     )
     slot_rank = jnp.sum((jnp.cumsum(one_hot, axis=0) - one_hot) * one_hot, axis=1)
-    slot_index = flat_expert * capacity + slot_rank
-    token_of = jnp.arange(2 * row_count, dtype=jnp.int32) // 2
-    outgoing = (
-        jnp.zeros((expert_count * capacity, width), jnp.bfloat16)
-        .at[slot_index]
-        .set(normed[token_of])
-    )
-    outgoing = outgoing.reshape(expert_count, capacity, width)
-    arrived = lax.all_to_all(outgoing, ("sp", "tp"), split_axis=0, concat_axis=0, tiled=True)
-    flat_rows = arrived.reshape(-1, width)
-    gate_out = jnp.dot(flat_rows, gate_weight[0], preferred_element_type=jnp.float32)
-    up_out = jnp.dot(flat_rows, up_weight[0], preferred_element_type=jnp.float32)
-    hidden = (jax.nn.silu(gate_out) * up_out).astype(jnp.bfloat16)
-    produced = jnp.dot(hidden, down_weight[0], preferred_element_type=jnp.float32).astype(
-        jnp.bfloat16
-    )
-    returned = lax.all_to_all(
-        produced.reshape(arrived.shape), ("sp", "tp"), split_axis=0, concat_axis=0, tiled=True
-    )
-    gathered = returned.reshape(expert_count * capacity, width)[slot_index].astype(jnp.float32)
-    weighted = gathered * route_weight.reshape(-1)[:, None]
-    combined = weighted.reshape(row_count, 2, width).sum(axis=1)
-    return (stream_f + combined).astype(jnp.bfloat16)
+    codes = (flat_expert * CAP + slot_rank).astype(jnp.float32).reshape(row_count, 2)
+    meta = jnp.concatenate(
+        [codes.T, route_weight.T, jnp.zeros((4, row_count), jnp.float32)], axis=0
+    )
+    return routed_experts(
+        normed, stream_f.astype(jnp.bfloat16), meta, gate_weight[0], up_weight[0], down_weight[0]
+    )
 
 
 def solution(mesh):

time: 330 us -> 264 us (0.80)
  Pallas kernels: 0 us -> 219 us
  blocking collectives: 129 us -> 0 us
  waiting for transfers between devices: 120 us -> 24 us
  local copies, waits for them, and re-layouts: 35.3 us -> 5.49 us
  starting transfers between devices: 18.9 us -> 6.53 us
  matrix products: 13.7 us -> 3.11 us
  other arithmetic: 11.4 us -> 5.26 us
    pallas_call x0 -> x1, Pallas kernels: none -> 219 us  [routed_experts(): pl.pallas_call(functools.partial(expert_kernel, ring, xs, tile), out_shap...]
    all_to_all x1 -> x0, blocking collectives: 129 us -> none  [per_device(): lax.all_to_all(outgoing, ('sp', 'tp'), split_axis=0, concat_axis=0, tiled...]
    all_to_all x1 -> x0, waiting for transfers between devices: 95.4 us -> none  [per_device(): lax.all_to_all(produced.reshape(arrived.shape), ('sp', 'tp'), split_axis=...]
    reshape x4 -> x0, local copies, waits for them, and re-layouts: 16.1 us -> none  [the longest x1 4.11 us: per_device(): produced.reshape(arrived.shape)]
    all_to_all x1 -> x0, starting transfers between devices: 12.4 us -> none  [per_device(): lax.all_to_all(produced.reshape(arrived.shape), ('sp', 'tp'), split_axis=...]
    dot_general x2 -> x0, matrix products: 10.7 us -> none  [the longest x1 6.22 us: per_device(): jnp.dot(hidden, down_weight[0], preferred_element_type=jnp.float32)]
    scatter x1 -> x0, local copies, waits for them, and re-layouts: 7 us -> none  [per_device(): outgoing = jnp.zeros((expert_count * capacity, width), jnp.bfloat16).at[s...]
    gather x1 -> x0, local copies, waits for them, and re-layouts: 5.2 us -> none  [per_device(): returned.reshape(expert_count * capacity, width)[slot_index]]
  transfers between devices with their start and end apart: 3 -> 2, of which waited for: 2 -> 1; matrix products, arithmetic and copies ran while one was open for 1% -> 1% of each run, Pallas kernels for 0% -> 0%
where the time goes in v1:
time: 264 us
  Pallas kernels  219 us (83%)
  waiting for transfers between devices  24 us (9%)
  starting transfers between devices  6.53 us (2%)
  local copies, waits for them, and re-layouts  5.49 us (2%)
  other arithmetic  5.26 us (2%)
  matrix products  3.11 us (1%)
    pallas_call x1, Pallas kernels, routed_experts(): pl.pallas_call(functools.partial(expert_kernel, ring, xs, tile), out_shap...  219 us
    all_to_all x1, waiting for transfers between devices, summed_on_arrival(): tiles = lax.all_to_all(cut_along(x, dim, size), axis, 0, 0, tiled=True)  24 us
  transfers between devices with their start and end apart: 2, of which 1 were waited for; matrix products, arithmetic and copies ran while one was open for 1% of the time, Pallas kernels for 0%

profile of v1, /device:TPU:40, one launch (start us, length us, event | category | flops | bytes accessed | tf_op | source)
XLA Modules:
  0.0 263.6 jit_solution(16955579921251318955)
XLA Ops:
  0.0 0.0 copy-start
  0.0 0.0 copy-start.3
  0.0 0.0 slice-start
  0.0 0.9 bitcast_convert_fusion
  1.0 0.3 fusion.29
  1.3 0.7 slice_bitcast_fusion.4
  2.1 1.8 collective-permute-start
  3.9 0.3 multiply_cosine_fusion
  4.3 1.1 copy.20
  5.4 0.1 convert.11
  5.4 0.1 add_compare_fusion
  5.5 0.2 broadcast_and_fusion
  5.7 0.1 subtract_convert_fusion
  5.8 0.0 copy-start.6
  5.9 0.0 copy-done.3
  5.9 0.0 slice-done
  6.0 0.0 collective-permute-done
  6.0 0.5 fusion.34
  6.5 0.0 copy-done.6
  6.5 0.1 broadcast_maximum_fusion
  6.6 0.3 fusion
  6.9 0.1 exponential_add_fusion
  7.0 0.5 fusion.1
  7.5 0.2 copy.23
  7.7 0.0 copy-done
  7.7 2.1 convolution_convert_fusion
  9.8 4.7 %all-to-all-start = ((bf16[4,128,2048]{2,1,0:T(8,128)(2,1)}), bf16[4,128,2048]{2,1,0:T(8,128)(2,1)S(1)}, u32[]{:S(2)}, u32[]{:S(2)}) async-start(bf16[4,128,2048]{2,1,0:T(8,128)(2,1)} %bitcast.91), calls=%async_computation | async-start | bytes 4194304 | tf_op jit(solution)/shard_map/all_to_all | solution.py:36
  14.5 0.0 copy-done.5
  14.5 0.1 copy.24
  14.6 0.1 eq.29
  14.8 0.1 eq.25
  14.9 0.1 copy.26
  15.0 0.2 fusion.10
  15.3 0.2 fusion.20
  15.5 0.1 reduce_sum.42
  15.7 0.1 copy.28
  15.7 0.1 pad.2.clone
  15.8 0.0 copy-done.7
  15.8 0.7 maximum_maximum_fusion.meta_ref
  16.5 24.0 %all-to-all-done = bf16[4,128,2048]{2,1,0:T(8,128)(2,1)S(1)} async-done(((bf16[4,128,2048]{2,1,0:T(8,128)(2,1)}), bf16[4,128,2048]{2,1,0:T(8,128)(2,1)S(1)}, u32[]{:S(2)}, u32[]{:S(2)}) %all-to-all-start) | async-done | bytes 2097184 | tf_op jit(solution)/shard_map/all_to_all | solution.py:36
  40.5 0.4 convert_reduce_fusion
  40.9 0.7 copy-done.2
  41.6 0.2 fusion.2
  41.8 0.0 copy-done.4
  41.8 1.0 fusion.4.normed_ref
  42.8 0.0 copy-done.1
  42.8 218.9 %shard_map.118 = bf16[128,2048]{1,0:T(8,128)(2,1)} custom-call(bf16[128,2048]{1,0:T(8,128)(2,1)} %fusion.4.normed_ref, bf16[128,2048]{1,0:T(8,128)(2,1)} %copy-done.1, f32[8,128]{1,0:T(8,128)} %maximum_maximum_fusion.meta_ref, bf16[2048,512]{1,0:T(8,128)(2,1)} %bitcast.92, bf16[2048,512]{1,0:T(8,128)(2,1)} %bitcast.93, bf16[512,2048]{1,0:T(8,128)(2,1)} %bitcast.94), custom_call_target="tpu_custom_call" | custom-call | tf_op jit(solution)/shard_map/pallas_call | solution.py:360
  261.7 1.9 copy.49
  (29 shorter events, 0.3 us)
Async XLA Ops:
  0.0 7.7 %copy-start = (bf16[256,2048]{1,0:T(8,128)(2,1)S(1)}, bf16[256,2048]{1,0:T(8,128)(2,1)}, u32[]{:S(2)}) copy-start(bf16[256,2048]{1,0:T(8,128)(2,1)} %param.17) | copy-start | bytes 3145732
  0.0 5.9 %copy-start.3 = (bf16[512,64]{0,1:T(8,128)(2,1)S(1)}, bf16[512,64]{0,1:T(8,128)(2,1)}, u32[]{:S(2)}) copy-start(bf16[512,64]{0,1:T(8,128)(2,1)} %param.14) | copy-start | bytes 196612
  0.0 5.9 %slice-start = ((bf16[512,64]{0,1:T(8,128)(2,1)}), bf16[384,64]{0,1:T(8,128)(2,1)S(1)}, s32[]{:S(2)}) async-start(bf16[512,64]{0,1:T(8,128)(2,1)} %param.14), calls=%async_computation.1 | async-start | bytes 98304 | tf_op jit(solution)/shard_map/slice | solution.py:429
  2.1 3.9 %collective-permute-start = (bf16[2,128,64]{1,2,0:T(8,128)(2,1)S(1)}, bf16[2,128,64]{1,2,0:T(8,128)(2,1)S(1)}, u32[]{:S(2)}, u32[]{:S(2)}) collective-permute-start(bf16[2,128,64]{1,2,0:T(8,128)(2,1)S(1)} %pad_maximum_fusion), channel_id=1, source_target_pairs={{0,4},{4,8},{8,12},{12,16},{16,20},{20,24},{24,28},{28,32},{32,36}... | collective-permute-start | bytes 98312 | tf_op jit(solution)/shard_map/ppermute | solution.py:25
  5.8 0.7 copy-start.6
  9.8 4.7 %copy-start.5 = (s32[128,2]{0,1:T(2,128)S(1)}, s32[128,2]{0,1:T(2,128)}, u32[]{:S(2)}) copy-start(s32[128,2]{0,1:T(2,128)} %param.22) | copy-start | bytes 3076
  9.8 6.0 %copy-start.7 = (f32[128,2]{0,1:T(2,128)S(1)}, f32[128,2]{0,1:T(2,128)}, u32[]{:S(2)}) copy-start(f32[128,2]{0,1:T(2,128)} %param.23) | copy-start | bytes 3076
  9.8 30.7 %all-to-all-start = ((bf16[4,128,2048]{2,1,0:T(8,128)(2,1)}), bf16[4,128,2048]{2,1,0:T(8,128)(2,1)S(1)}, u32[]{:S(2)}, u32[]{:S(2)}) async-start(bf16[4,128,2048]{2,1,0:T(8,128)(2,1)} %bitcast.91), calls=%async_computation | async-start | bytes 4194304 | tf_op jit(solution)/shard_map/all_to_all | solution.py:36
  16.5 25.3 %copy-start.4 = (f32[2048]{0:T(1024)S(1)}, f32[2048]{0:T(1024)}, u32[]{:S(2)}) copy-start(f32[2048]{0:T(1024)} %param.18) | copy-start | bytes 24580
  40.5 1.0 copy-start.2
  41.8 1.0 copy-start.1

commit v2 on v1

--- a/solution.py
+++ b/solution.py
@@ -8,61 +8,43 @@
 from jax.sharding import PartitionSpec as P
 
 MESH_ID = pl.DeviceIdType.MESH
+HDIM = 64
+WINDOW = 128
 CAP = 4
 CORES = 2
 
-HDIM = 64
-WINDOW = 128
-
 
 rope_base = 10000.0
 norm_eps = 1e-06
-
-
-def shifted(block, axis, distance):
-    devices = range(lax.axis_size(axis))
-    route = [(i - distance, i) for i in devices if i - distance in devices]
-    return lax.ppermute(block, axis, route)
-
-
-def cut_along(x, dim, size):
-    lengths = x.shape
-    tiles = x.reshape(*lengths[:dim], size, lengths[dim] // size, *lengths[dim + 1 :])
-    return jnp.moveaxis(tiles, dim, 0)
-
-
-def summed_on_arrival(x, axis, dim):
-    size = lax.axis_size(axis)
-    tiles = lax.all_to_all(cut_along(x, dim, size), axis, 0, 0, tiled=True)
-    return jnp.sum(tiles.astype(jnp.float32), axis=0)
-
-
-def rotate(rows, positions, heads):
-    half_dim = HDIM // 2
-    values = rows.astype(jnp.float32).reshape(rows.shape[0], heads, HDIM)
-    inverse = rope_base ** (-jnp.arange(half_dim, dtype=jnp.float32) / half_dim)
-    angles = positions.astype(jnp.float32)[:, None] * inverse[None, :]
-    cosines = jnp.cos(angles)[:, None, :]
-    sines = jnp.sin(angles)[:, None, :]
-    lower = values[..., :half_dim]
-    upper = values[..., half_dim:]
-    turned = jnp.concatenate(
-        [lower * cosines - upper * sines, upper * cosines + lower * sines], axis=-1
-    )
-    return turned.reshape(rows.shape[0], heads * HDIM).astype(jnp.bfloat16)
 
 
 def expert_kernel(
     ring,
     xs,
     tile,
-    normed_ref,
-    stream_ref,
+    query_ref,
+    key_ref,
+    value_ref,
+    cos_ref,
+    sin_ref,
+    sink_ref,
+    gain_ref,
     meta_ref,
+    residual_hbm,
+    proj_hbm,
     gate_hbm,
     up_hbm,
     down_hbm,
     out_ref,
+    rot_q,
+    keys_values,
+    residual,
+    proj_w,
+    shares,
+    far_in,
+    near_in,
+    own_share_sum,
+    stream,
     pool,
     pool_meta,
     picked,
@@ -87,9 +69,15 @@
     back_recv,
     sum_send,
     sum_recv,
+    halo_send,
+    halo_recv,
+    far_send,
+    far_recv,
+    near_send,
+    near_recv,
 ):
     f32, bf16 = jnp.float32, jnp.bfloat16
-    rows, width = normed_ref.shape
+    rows, width = residual.shape
     half = rows // 2
     far = ring // 2
     peers = xs * CORES
@@ -106,7 +94,15 @@
 
     loads = [
         pltpu.make_async_copy(src, dst, weight_sem.at[i])
-        for i, (src, dst) in enumerate(((gate_hbm, gate_w), (up_hbm, up_w), (down_hbm, down_w)))
+        for i, (src, dst) in enumerate(
+            (
+                (proj_hbm, proj_w),
+                (residual_hbm, residual),
+                (gate_hbm, gate_w),
+                (up_hbm, up_w),
+                (down_hbm, down_w),
+            )
+        )
     ]
     for load in loads:
         load.start()
@@ -114,19 +110,50 @@
     barrier = pltpu.get_barrier_semaphore()
     pl.semaphore_signal(barrier, inc=1, device_id=nxt, device_id_type=MESH_ID)
     pl.semaphore_signal(barrier, inc=1, device_id=prv, device_id_type=MESH_ID)
+    total_sp = ring * CORES
+    after = {"sp": lax.rem(sp + 1, total_sp)}
+    across = {"sp": lax.rem(sp + jnp.where(core == 1, 1, total_sp - 1), total_sp)}
+    pl.semaphore_signal(barrier, inc=1, device_id=across, device_id_type=MESH_ID)
     for o in range(1, peers):
         pl.semaphore_signal(barrier, inc=1, device_id=peer(o)[1], device_id_type=MESH_ID)
-    pl.semaphore_wait(barrier, peers + 1)
+
+    lane = lax.broadcasted_iota(jnp.int32, (query_ref.shape[1],) * 2, 1)
+    line = lax.broadcasted_iota(jnp.int32, (query_ref.shape[1],) * 2, 0)
+    low = lax.rem(lane, HDIM) < HDIM // 2
+    turn = jnp.where(low & (line == lane + HDIM // 2), -1.0, 0.0)
+    turn = (turn + jnp.where((~low) & (line == lane - HDIM // 2), 1.0, 0.0)).astype(bf16)
+
+    def rotated(x, cosines, sines):
+        n = x.shape[1]
+        swapped = jnp.dot(x, turn[:n, :n], preferred_element_type=f32)
+        return (x.astype(f32) * cosines + swapped * sines).astype(bf16)
+
+    tok = query_ref.shape[0]
+    keys_values[WINDOW:, 0:HDIM] = rotated(key_ref[...], cos_ref[:, 0:HDIM], sin_ref[:, 0:HDIM])
+    keys_values[WINDOW:, HDIM:] = value_ref[...]
+    pl.semaphore_wait(barrier, peers + 2)
+    halo = pltpu.make_async_remote_copy(
+        src_ref=keys_values.at[pl.ds(tok, WINDOW)],
+        dst_ref=keys_values.at[pl.ds(0, WINDOW)],
+        send_sem=halo_send,
+        recv_sem=halo_recv,
+        device_id=after,
+        device_id_type=MESH_ID,
+    )
+    halo.start()
+    for c in range(query_ref.shape[1] // 128):
+        cols = pl.ds(c * 128, 128)
+        rot_q[:, cols] = rotated(query_ref[:, cols], cos_ref[...], sin_ref[...])
+    halo.wait_recv()
 
     def part(h):
         return pl.ds(h * half, half)
 
-    def send_pool(way, slot, h, src=None):
+    def send_pool(way, slot, h):
         to = slot + 1 if way == 0 else lax.rem(slot + ring - 1, ring)
         step = slot if way == 0 else lax.rem(ring - slot, ring)
-        src = pool.at[slot, part(h)] if src is None else src
         return pltpu.make_async_remote_copy(
-            src_ref=src,
+            src_ref=pool.at[slot, part(h)],
             dst_ref=pool.at[to, part(h)],
             send_sem=pool_send.at[way, step, h],
             recv_sem=pool_recv.at[way, step, h],
@@ -148,10 +175,96 @@
 
     for way in range(2):
         send_meta(way, 0, meta_ref).start()
+    pool_meta[0] = meta_ref[...]
+
+    q_at = lax.broadcasted_iota(jnp.int32, (WINDOW, 2 * WINDOW), 0)
+    k_at = lax.broadcasted_iota(jnp.int32, (WINDOW, 2 * WINDOW), 1)
+    reach = q_at + WINDOW - k_at
+
+    def projected(block):
+        start = pl.multiple_of(block * WINDOW, WINDOW)
+        first = start + sp * tok
+        allowed = (reach >= 0) & (reach < WINDOW) & (k_at + first >= WINDOW)
+        kv = keys_values[pl.ds(start, 2 * WINDOW), :]
+        k, v = kv[:, 0:HDIM], kv[:, HDIM:]
+        q = rot_q[pl.ds(start, WINDOW), :]
+        heads = []
+        for h in range(q.shape[1] // HDIM):
+            qh = q[:, h * HDIM : (h + 1) * HDIM]
+            s = lax.dot_general(qh, k, (((1,), (1,)), ((), ())), preferred_element_type=f32)
+            s = jnp.where(allowed, s * HDIM ** (-0.5), -jnp.inf)
+            sink = sink_ref[h]
+            top = jnp.maximum(jnp.max(s, axis=1, keepdims=True), sink)
+            e = jnp.exp(s - top)
+            below = jnp.sum(e, axis=1, keepdims=True) + jnp.exp(sink - top)
+            p = (e / below).astype(bf16)
+            heads.append(jnp.dot(p, v, preferred_element_type=f32).astype(bf16))
+        att = jnp.concatenate(heads, axis=1)
+        for c in range(width // tile):
+            cols = pl.ds(c * tile, tile)
+            yield cols, jnp.dot(att, proj_w[:, cols], preferred_element_type=f32)
+
+    def beside(step):
+        return {"tp": lax.rem(tp + step + xs, xs)}
+
+    quarter = half // 2
+
+    def send_far(way, h):
+        at = h * half + way * quarter
+        return pltpu.make_async_remote_copy(
+            src_ref=shares.at[2, pl.ds(at, quarter)],
+            dst_ref=far_in.at[way, h],
+            send_sem=far_send.at[way, h],
+            recv_sem=far_recv.at[way, h],
+            device_id=beside(1 - 2 * way),
+            device_id_type=MESH_ID,
+        )
+
+    def send_near(way, h):
+        return pltpu.make_async_remote_copy(
+            src_ref=shares.at[way, part(h)],
+            dst_ref=near_in.at[way, h],
+            send_sem=near_send.at[way, h],
+            recv_sem=near_recv.at[way, h],
+            device_id=beside(1 - 2 * way),
+            device_id_type=MESH_ID,
+        )
+
+    loads[0].wait()
+    for cols, y in projected(lax.rem(tp + 2, xs)):
+        shares[2, :, cols] = y.astype(bf16)
+    for h in range(2):
+        for way in range(2):
+            send_far(way, h).start()
+    for way in range(2):
+        for cols, y in projected(lax.rem(tp + 1 - 2 * way + xs, xs)):
+            own_share_sum[:, cols] = y
         for h in range(2):
-            send_pool(way, 0, h, normed_ref.at[part(h)]).start()
-    pool[0] = normed_ref[...]
-    pool_meta[0] = meta_ref[...]
+            send_far(way, h).wait_recv()
+            joint = pl.ds(h * half + way * quarter, quarter)
+            alone = pl.ds(h * half + (1 - way) * quarter, quarter)
+            shares[way, alone] = own_share_sum[alone].astype(bf16)
+            joined = own_share_sum[joint] + far_in[way, h].astype(f32)
+            shares[way, joint] = joined.astype(bf16)
+            send_near(way, h).start()
+    for cols, y in projected(tp):
+        own_share_sum[:, cols] = y
+    loads[1].wait()
+
+    def own_rows(h):
+        for way in range(2):
+            send_near(way, h).wait_recv()
+        got = near_in[0, h].astype(f32) + near_in[1, h].astype(f32)
+        x = residual[part(h)].astype(f32) + (own_share_sum[part(h)] + got)
+        x = x.astype(bf16)
+        stream[part(h)] = x
+        x = x.astype(f32)
+        scale = lax.rsqrt(jnp.mean(x * x, axis=1, keepdims=True) + norm_eps)
+        pool[0, part(h)] = (x * scale * gain_ref[...]).astype(bf16)
+        for way in range(2):
+            send_pool(way, 0, h).start()
+
+    own_rows(0)
 
     row_id = lax.broadcasted_iota(jnp.int32, (peers * 2 * CAP, rows), 0)
     local_code = (row_id // (2 * CAP)) * CAP + lax.rem(row_id, CAP)
@@ -235,6 +348,10 @@
                 def _():
                     send_meta(1, ring - n).start()
 
+                @pl.when(n == 1)
+                def _():
+                    own_rows(1)
+
                 @pl.when(n >= 2)
                 def _():
                     serve(n - 2)
@@ -242,7 +359,7 @@
                 pick(n - 1)
         return 0
 
-    for load in loads:
+    for load in loads[2:]:
         load.wait()
     lax.fori_loop(1, far, ring_step, 0)
     serve(far - 2)
@@ -312,7 +429,7 @@
 
     lax.fori_loop(0, far - 1, sum_step, 0)
     own_share(0, 0, False, left_own)
-    left_own[...] += stream_ref[...].astype(f32)
+    left_own[...] += stream[...].astype(f32)
     for h in (1, 0):
         send_sum(0, 1, h).wait_recv()
         send_sum(1, 1, h).wait_recv()
@@ -342,41 +459,56 @@
         return 0
 
     lax.fori_loop(0, far, drain, 0)
-
-
-def routed_experts(normed, stream, meta, gate, up, down):
-    rows, width = normed.shape
+    halo.wait_send()
+    for h in range(2):
+        for way in range(2):
+            send_far(way, h).wait_send()
+            send_near(way, h).wait_send()
+
+
+def layer(query, key, value, cosines, sines, sinks, gain, meta, residual, proj, gate, up, down):
+    rows, width = residual.shape
     ring = lax.axis_size("sp") // CORES
     xs = lax.axis_size("tp")
     far = ring // 2
     peers = xs * CORES
     hidden = gate.shape[1]
     tile = min(512, width)
-    bf16 = jnp.bfloat16
+    bf16, f32 = jnp.bfloat16, jnp.float32
     vmem = pl.BlockSpec(memory_space=pltpu.VMEM)
+    smem = pl.BlockSpec(memory_space=pltpu.SMEM)
     hbm = pl.BlockSpec(memory_space=pl.ANY)
     slab = (far, peers, 2 * CAP, width)
     dma = pltpu.SemaphoreType.DMA
     return pl.pallas_call(
         functools.partial(expert_kernel, ring, xs, tile),
         out_shape=jax.ShapeDtypeStruct((rows, width), bf16),
-        in_specs=[vmem, vmem, vmem, hbm, hbm, hbm],
+        in_specs=[vmem] * 5 + [smem] + [vmem] * 2 + [hbm] * 5,
         out_specs=vmem,
         scratch_shapes=[
+            pltpu.VMEM(query.shape, bf16),
+            pltpu.VMEM((query.shape[0] + WINDOW, 2 * HDIM), bf16),
+            pltpu.VMEM((rows, width), bf16),
+            pltpu.VMEM(proj.shape, bf16),
+            pltpu.VMEM((3, rows, width), bf16),
+            pltpu.VMEM((2, 2, rows // 4, width), bf16),
+            pltpu.VMEM((2, 2, rows // 2, width), bf16),
+            pltpu.VMEM((rows, width), f32),
+            pltpu.VMEM((rows, width), bf16),
             pltpu.VMEM((ring, rows, width), bf16),
-            pltpu.VMEM((ring, 8, rows), jnp.float32),
+            pltpu.VMEM((ring, 8, rows), f32),
             pltpu.VMEM(slab, bf16),
             pltpu.VMEM(slab, bf16),
             pltpu.VMEM(slab, bf16),
             pltpu.VMEM(slab, bf16),
             pltpu.VMEM((far + 1, rows, width), bf16),
             pltpu.VMEM((far + 1, rows, width), bf16),
-            pltpu.VMEM((rows, width), jnp.float32),
-            pltpu.VMEM((rows, width), jnp.float32),
+            pltpu.VMEM((rows, width), f32),
+            pltpu.VMEM((rows, width), f32),
             pltpu.VMEM((width, hidden), bf16),
             pltpu.VMEM((width, hidden), bf16),
             pltpu.VMEM((hidden, width), bf16),
-            dma((3,)),
+            dma((5,)),
             dma((2, far, 2)),
             dma((2, far, 2)),
             dma((2, far)),
@@ -387,11 +519,17 @@
             dma((far, peers)),
             dma((2, far, 2)),
             dma((2, far, 2)),
+            dma,
+            dma,
+            dma((2, 2)),
+            dma((2, 2)),
+            dma((2, 2)),
+            dma((2, 2)),
         ],
         compiler_params=pltpu.CompilerParams(
             collective_id=1, has_side_effects=True, vmem_limit_bytes=60 * 1024 * 1024
         ),
-    )(normed, stream, meta, gate, up, down)
+    )(query, key, value, cosines, sines, sinks, gain, meta, residual, proj, gate, up, down)
 
 
 def per_device(
@@ -409,59 +547,13 @@
     route_weight,
 ):
     tok_count = query_rows.shape[0]
-    head_local = query_rows.shape[1] // HDIM
-    group_local = key_rows.shape[1] // HDIM
-    repeat = head_local // group_local
-    first_pos = lax.axis_index("sp") * tok_count
-    positions = first_pos + jnp.arange(tok_count, dtype=jnp.int32)
-    rot_q = rotate(query_rows, positions, head_local)
-    rot_k = rotate(key_rows, positions, group_local)
-    tails = jnp.stack([rot_k[tok_count - WINDOW :], value_rows[tok_count - WINDOW :]])
-    earlier = shifted(tails, "sp", 1)
-    blocks = tok_count // WINDOW
-    q_blocks = rot_q.reshape(blocks, WINDOW, group_local, repeat, HDIM)
-    k_blocks = rot_k.reshape(blocks, WINDOW, group_local, HDIM)
-    v_blocks = value_rows.reshape(blocks, WINDOW, group_local, HDIM)
-    k_prev = jnp.concatenate(
-        [earlier[0].reshape(1, WINDOW, group_local, HDIM), k_blocks[:-1]], axis=0
-    )
-    v_prev = jnp.concatenate(
-        [earlier[1].reshape(1, WINDOW, group_local, HDIM), v_blocks[:-1]], axis=0
-    )
-    k_wide = jnp.concatenate([k_prev, k_blocks], axis=1)
-    v_wide = jnp.concatenate([v_prev, v_blocks], axis=1)
-    query_pos = jnp.arange(WINDOW) + WINDOW
-    key_pos = jnp.arange(2 * WINDOW)
-    distance = query_pos[:, None] - key_pos[None, :]
-    in_band = (distance >= 0) & (distance < WINDOW)
-    key_global = (
-        first_pos + jnp.arange(blocks)[:, None, None] * WINDOW + key_pos[None, None, :] - WINDOW
-    )
-    allowed = in_band[None] & (key_global >= 0)
-    scores = jnp.einsum(
-        "nqgrd,nkgd->grnqk", q_blocks, k_wide, preferred_element_type=jnp.float32
-    ) * HDIM ** (-0.5)
-    scores = jnp.where(allowed[None, None], scores, -jnp.inf)
-    sink_here = sink_logits.reshape(group_local, repeat)[:, :, None, None, None]
-    largest = jnp.maximum(scores.max(axis=-1, keepdims=True), sink_here)
-    exp_scores = jnp.exp(scores - largest)
-    denominator = exp_scores.sum(axis=-1, keepdims=True) + jnp.exp(sink_here - largest)
-    probs = (exp_scores / denominator).astype(jnp.bfloat16)
-    attended = jnp.einsum("grnqk,nkgd->nqgrd", probs, v_wide, preferred_element_type=jnp.float32)
-    attended = attended.astype(jnp.bfloat16).reshape(tok_count, head_local * HDIM)
     row_count = residual.shape[0]
-    projected = summed_on_arrival(
-        jnp.dot(attended, out_weight, preferred_element_type=jnp.float32).astype(jnp.bfloat16),
-        "tp",
-        0,
-    )
-    stream_f = (residual.astype(jnp.float32) + projected).astype(jnp.bfloat16).astype(jnp.float32)
-    normed = (
-        stream_f
-        * lax.rsqrt(jnp.mean(stream_f * stream_f, axis=-1, keepdims=True) + norm_eps)
-        * norm_gain[None, :]
-    ).astype(jnp.bfloat16)
-    width = normed.shape[1]
+    positions = lax.axis_index("sp") * tok_count + jnp.arange(tok_count, dtype=jnp.int32)
+    half_dim = HDIM // 2
+    inverse = rope_base ** (-jnp.arange(half_dim, dtype=jnp.float32) / half_dim)
+    angles = positions.astype(jnp.float32)[:, None] * inverse[None, :]
+    cosines = jnp.tile(jnp.cos(angles), (1, 128 // half_dim))
+    sines = jnp.tile(jnp.sin(angles), (1, 128 // half_dim))
     expert_count = lax.axis_size("sp") * lax.axis_size("tp")
     flat_expert = routes.reshape(-1)
     one_hot = (flat_expert[:, None] == jnp.arange(expert_count, dtype=jnp.int32)[None, :]).astype(
@@ -472,8 +564,20 @@
     meta = jnp.concatenate(
         [codes.T, route_weight.T, jnp.zeros((4, row_count), jnp.float32)], axis=0
     )
-    return routed_experts(
-        normed, stream_f.astype(jnp.bfloat16), meta, gate_weight[0], up_weight[0], down_weight[0]
+    return layer(
+        query_rows,
+        key_rows,
+        value_rows,
+        cosines,
+        sines,
+        sink_logits,
+        norm_gain[None, :],
+        meta,
+        residual,
+        out_weight,
+        gate_weight[0],
+        up_weight[0],
+        down_weight[0],
     )
 
 

time: 264 us -> 253 us (0.958)
  waiting for transfers between devices: 24 us -> 0 us
  Pallas kernels: 219 us -> 241 us
  starting transfers between devices: 6.53 us -> 0 us
  matrix products: 3.11 us -> 0 us
  local copies, waits for them, and re-layouts: 5.49 us -> 8.28 us
    all_to_all x1 -> x0, waiting for transfers between devices: 24 us -> none  [summed_on_arrival(): tiles = lax.all_to_all(cut_along(x, dim, size), axis, 0, 0, tiled=True)]
    pallas_call x1, Pallas kernels: 219 us -> 241 us  [layer(): pl.pallas_call(functools.partial(expert_kernel, ring, xs, tile), out_shap...]
    all_to_all x1 -> x0, starting transfers between devices: 4.71 us -> none  [summed_on_arrival(): tiles = lax.all_to_all(cut_along(x, dim, size), axis, 0, 0, tiled=True)]
    dot_general x3 -> x0, matrix products: 3.11 us -> none  [the longest x1 2.1 us: per_device(): jnp.dot(attended, out_weight, preferred_element_type=jnp.float32)]
    unnamed x20 -> x5, local copies, waits for them, and re-layouts: 3.77 us -> 5.88 us
  transfers between devices with their start and end apart: 2 -> 0, of which waited for: 1 -> 0; matrix products, arithmetic and copies ran while one was open for 1% -> 0% of each run, Pallas kernels for 0% -> 0%
where the time goes in v2:
time: 253 us; the launch traced here: 252 us
  Pallas kernels  241 us (95%)
  local copies, waits for them, and re-layouts  8.28 us (3%)
  other arithmetic  2.8 us (1%)
    pallas_call x1, Pallas kernels, layer(): pl.pallas_call(functools.partial(expert_kernel, ring, xs, tile), out_shap...  241 us
    unnamed x5, local copies, waits for them, and re-layouts  5.88 us

profile of v2, /device:TPU:40, one launch (start us, length us, event | category | flops | bytes accessed | tf_op | source)
XLA Modules:
  0.0 251.9 jit_solution(729077730110037953)
XLA Ops:
  0.0 0.1 pad.2.clone
  0.1 0.8 copy.15
  0.9 0.1 eq.29
  1.0 0.1 eq.25
  1.2 0.1 copy.17
  1.3 0.2 fusion
  1.6 0.2 fusion.2
  1.8 0.1 reduce_sum.12
  1.9 0.1 copy.19
  2.0 0.7 convert_bitcast_fusion
  2.7 1.3 maximum_maximum_fusion.meta_ref
  4.0 0.3 multiply_sine_fusion
  4.3 1.6 copy.20.key_ref
  5.9 1.6 copy.21.value_ref
  7.6 0.8 copy.23.sin_ref
  8.4 0.8 copy.22.cos_ref
  9.3 240.8 %shard_map.118 = bf16[128,2048]{1,0:T(8,128)(2,1)} custom-call(bf16[512,256]{1,0:T(8,128)(2,1)} %query_ref.1, bf16[512,64]{1,0:T(8,128)(2,1)} %copy.20.key_ref, bf16[512,64]{1,0:T(8,128)(2,1)} %copy.21.value_ref, f32[512,128]{1,0:T(8,128)} %copy.22.cos_ref, f32[512,128]{1,0:T(8,128)} %copy.23.sin_ref, f32[4]{0:T(128)} %sink_ref.1, f32[1,2048]{1,0:T(1,128)} %bitcast.30, ...), custom_call_target="tpu_custom_call" | custom-call | tf_op jit(solution)/shard_map/pallas_call | solution.py:483
  250.1 1.9 copy.25
  (11 shorter events, 0.1 us)

commit v3 on v2

--- a/solution.py
+++ b/solution.py
@@ -12,6 +12,12 @@
 WINDOW = 128
 CAP = 4
 CORES = 2
+EXPERTS_PER_GROUP = 32
+SPAN = 4
+FIRST = (0, 4, 12)
+LAST = (3, 7, 9)
+ENTRIES = 22
+HOME = 22
 
 
 rope_base = 10000.0
@@ -29,7 +35,8 @@
     sin_ref,
     sink_ref,
     gain_ref,
-    meta_ref,
+    ids_ref,
+    mix_ref,
     residual_hbm,
     proj_hbm,
     gate_hbm,
@@ -45,16 +52,17 @@
     near_in,
     own_share_sum,
     stream,
+    normed,
+    places,
+    sums,
+    total,
     pool,
     pool_meta,
     picked,
     routed,
     made,
     back,
-    left_sum,
-    right_sum,
-    left_own,
-    right_own,
+    own_part,
     gate_w,
     up_w,
     down_w,
@@ -149,33 +157,89 @@
     def part(h):
         return pl.ds(h * half, half)
 
-    def send_pool(way, slot, h):
-        to = slot + 1 if way == 0 else lax.rem(slot + ring - 1, ring)
-        step = slot if way == 0 else lax.rem(ring - slot, ring)
+    block, at = z // SPAN, lax.rem(z, SPAN)
+    opposite_way = jnp.where(at >= SPAN // 2, 0, 1)
+    ends = (at, SPAN - 1 - at)
+    onward = (nxt, prv)
+    room = 2 * peers * CAP
+
+    def origin(way, d):
+        i = lax.rem(ends[way] - d + 3 * SPAN, SPAN)
+        return i, (d + i - ends[way]) // SPAN
+
+    def passes(way, kind, d):
+        i, crossed = origin(way, d)
+        there = (d <= LAST[kind]) & (kind >= crossed)
+        return there & (i >= SPAN // 2) if kind == 2 else there
+
+    def is_mine(way, kind, d):
+        return origin(way, d)[1] == kind
+
+    def send_chunk(way, kind, d, count):
+        entry = FIRST[kind] + d
         return pltpu.make_async_remote_copy(
-            src_ref=pool.at[slot, part(h)],
-            dst_ref=pool.at[to, part(h)],
-            send_sem=pool_send.at[way, step, h],
-            recv_sem=pool_recv.at[way, step, h],
-            device_id=nxt if way == 0 else prv,
+            src_ref=pool.at[way, entry, pl.ds(0, count)],
+            dst_ref=pool.at[way, entry + 1, pl.ds(0, count)],
+            send_sem=pool_send.at[way, entry],
+            recv_sem=pool_recv.at[way, entry + 1],
+            device_id=onward[way],
             device_id_type=MESH_ID,
         )
 
-    def send_meta(way, slot, src=None):
-        to = slot + 1 if way == 0 else lax.rem(slot + ring - 1, ring)
-        step = slot if way == 0 else lax.rem(ring - slot, ring)
+    def send_meta(way, kind, d):
+        entry = FIRST[kind] + d
         return pltpu.make_async_remote_copy(
-            src_ref=pool_meta.at[slot] if src is None else src,
-            dst_ref=pool_meta.at[to],
-            send_sem=meta_send.at[way, step],
-            recv_sem=meta_recv.at[way, step],
-            device_id=nxt if way == 0 else prv,
+            src_ref=pool_meta.at[way, entry],
+            dst_ref=pool_meta.at[way, entry + 1],
+            send_sem=meta_send.at[way, entry],
+            recv_sem=meta_recv.at[way, entry + 1],
+            device_id=onward[way],
             device_id_type=MESH_ID,
         )
 
-    for way in range(2):
-        send_meta(way, 0, meta_ref).start()
-    pool_meta[0] = meta_ref[...]
+    def forwards(way, kind, d):
+        goes = passes(way, kind, d)
+        mine_here = is_mine(way, kind, d)
+        whole = goes & jnp.where(mine_here, ends[way] < SPAN - 2, True)
+        return whole, goes & mine_here & (ends[way] == SPAN - 2)
+
+    def forward(way, kind, d, act):
+        whole, first = forwards(way, kind, d)
+
+        @pl.when(whole)
+        def _():
+            act(send_chunk(way, kind, d, room), send_meta(way, kind, d))
+
+        @pl.when(first)
+        def _():
+            act(send_chunk(way, kind, d, room // 2), send_meta(way, kind, d))
+
+    def start_both(chunk, about):
+        about.start()
+        chunk.start()
+
+    def wait_sent(chunk, about):
+        about.wait_send()
+        chunk.wait_send()
+
+    def receive(way, kind, d):
+        goes = passes(way, kind, d)
+        short = is_mine(way, kind, d) & (ends[way] == SPAN - 1)
+
+        @pl.when(goes)
+        def _():
+            send_meta(way, kind, d - 1).wait_recv()
+
+        @pl.when(goes & ~short)
+        def _():
+            send_chunk(way, kind, d - 1, room).wait_recv()
+
+        @pl.when(goes & short)
+        def _():
+            send_chunk(way, kind, d - 1, room // 2).wait_recv()
+            pool[way, FIRST[kind] + d, pl.ds(room // 2, room // 2)] = jnp.zeros(
+                (room // 2, width), bf16
+            )
 
     q_at = lax.broadcasted_iota(jnp.int32, (WINDOW, 2 * WINDOW), 0)
     k_at = lax.broadcasted_iota(jnp.int32, (WINDOW, 2 * WINDOW), 1)
@@ -260,28 +324,120 @@
         stream[part(h)] = x
         x = x.astype(f32)
         scale = lax.rsqrt(jnp.mean(x * x, axis=1, keepdims=True) + norm_eps)
-        pool[0, part(h)] = (x * scale * gain_ref[...]).astype(bf16)
-        for way in range(2):
-            send_pool(way, 0, h).start()
+        normed[part(h)] = (x * scale * gain_ref[...]).astype(bf16)
+
+    ids = ids_ref[...]
+    expert_at = lax.broadcasted_iota(jnp.int32, (ring * peers, rows), 0)
+    token_row = lax.broadcasted_iota(jnp.int32, (rows, rows), 0)
+    token_col = lax.broadcasted_iota(jnp.int32, (rows, rows), 1)
+    ahead = (token_row < token_col).astype(f32).astype(bf16)
+    named = [(expert_at == ids[c : c + 1]).astype(f32) for c in range(2)]
+    earlier = jnp.dot((named[0] + named[1]).astype(bf16), ahead, preferred_element_type=f32)
+    ranks = [jnp.sum(n * earlier, axis=0, keepdims=True) for n in named]
+    group = ids[0:1] // EXPERTS_PER_GROUP
+    chip = [ids[c : c + 1] // peers for c in range(2)]
+    spot = [lax.rem(c, SPAN) for c in chip]
+    blocks = ring // SPAN
+    apart = lax.rem(group - block + blocks, blocks)
+    top = [(spot[0] == SPAN - 1) | (spot[1] == SPAN - 1), (spot[0] == 0) | (spot[1] == 0)]
+    beyond = [(spot[0] > at) | (spot[1] > at), (spot[0] < at) | (spot[1] < at)]
+    here = (chip[0] == z) | (chip[1] == z)
+    joins = [
+        (apart == 0) & beyond[0],
+        apart == 1,
+        (apart == 0) & beyond[1],
+        apart == blocks - 1,
+        apart == 2,
+        here,
+    ]
+    joins = [x.astype(f32) for x in joins]
+    top = [x.astype(f32) for x in top]
+    leads = [top[0], top[0], top[1], top[1], jnp.where(at >= SPAN // 2, top[0], top[1]), top[0]]
+    pack_row = lax.broadcasted_iota(jnp.int32, (8, rows), 0)
+    lead, rest = jnp.zeros((8, rows), f32), jnp.zeros((8, rows), f32)
+    for n in range(6):
+        lead = jnp.where(pack_row == n, joins[n] * leads[n], lead)
+        rest = jnp.where(pack_row == n, joins[n] * (1.0 - leads[n]), rest)
+    lead_rank = jnp.dot(lead.astype(bf16), ahead, preferred_element_type=f32)
+    rest_rank = jnp.dot(rest.astype(bf16), ahead, preferred_element_type=f32)
+    rest_rank += jnp.sum(lead, axis=1, keepdims=True)
+    places[...] = jnp.where(lead > 0, lead_rank, jnp.where(rest > 0, rest_rank, -1.0))
+    mix = mix_ref[...]
+    mix_high = mix.astype(bf16).astype(f32)
+    mix_low = mix - mix_high
+    facts_row = lax.broadcasted_iota(jnp.int32, (16, rows), 0)
+    facts = jnp.where(facts_row == 8, 1.0, 0.0)
+    known = [ids[0:1].astype(f32), ids[1:2].astype(f32), ranks[0], ranks[1]]
+    known += [mix_high[0:1], mix_high[1:2], mix_low[0:1], mix_low[1:2]]
+    for n in range(8):
+        facts = jnp.where(facts_row == n, known[n], facts)
+    facts = facts.astype(bf16)
+    chunk_row = lax.broadcasted_iota(jnp.int32, (room, rows), 0).astype(f32)
+
+    def packing(n):
+        return (chunk_row == places[n : n + 1, :]).astype(f32).astype(bf16)
+
+    def pack(n, way, entry):
+        choose = packing(n)
+        for c in range(width // tile):
+            cols = pl.ds(c * tile, tile)
+            got = jnp.dot(choose, normed[:, cols], preferred_element_type=f32)
+            pool[way, entry, :, cols] = got.astype(bf16)
+
+    def pack_meta(n, way, entry):
+        got = lax.dot_general(
+            facts, packing(n), (((1,), (1,)), ((), ())), preferred_element_type=f32
+        )
+        out_row = lax.broadcasted_iota(jnp.int32, (8, room), 0)
+        found = got[8:9] > 0
+        out = jnp.where(out_row == 0, jnp.where(found, got[0:1] * CAP + got[2:3], -1.0), 0.0)
+        out = jnp.where(out_row == 1, jnp.where(found, got[1:2] * CAP + got[3:4], -1.0), out)
+        out = jnp.where(out_row == 2, got[4:5] + got[6:7], out)
+        out = jnp.where(out_row == 3, got[5:6] + got[7:8], out)
+        pool_meta[way, entry] = jnp.concatenate([out, jnp.zeros_like(out)], axis=1)
+
+    packs = ((4, opposite_way, 2), (1, 0, 1), (3, 1, 1), (0, 0, 0), (2, 1, 0))
+    for n, way, kind in packs:
+        pack_meta(n, way, FIRST[kind])
+    pack_meta(5, 0, HOME)
 
     own_rows(0)
-
-    row_id = lax.broadcasted_iota(jnp.int32, (peers * 2 * CAP, rows), 0)
+    own_rows(1)
+    for n, way, kind in packs:
+        pack(n, way, FIRST[kind])
+        if kind == 2:
+            for w in range(2):
+                forward(w, 2, 0, start_both)
+        else:
+            forward(way, kind, 0, start_both)
+    pack(5, 0, HOME)
+
+    row_id = lax.broadcasted_iota(jnp.int32, (room, room), 0)
     local_code = (row_id // (2 * CAP)) * CAP + lax.rem(row_id, CAP)
-    in_second = lax.rem(row_id, 2 * CAP) >= CAP
+    which_half = lax.rem(row_id, 2 * CAP) // CAP
     base = z * (peers * CAP)
 
-    def matches(slot, second):
-        here = jnp.where(in_second == second, local_code + base, -1).astype(f32)
-        m = pool_meta[slot]
-        return here == m[0:1, :], here == m[1:2, :], m
-
-    def pick_of(slot, second):
-        first_hit, second_hit, _ = matches(slot, second)
+    def locate(back):
+        other = back > at + SPAN + SPAN // 2
+        d = jnp.where(other, ring - back, back)
+        end = jnp.where(other, ends[1], ends[0])
+        i = lax.rem(end - d + 3 * SPAN, SPAN)
+        crossed = (d + i - end) // SPAN
+        first = jnp.where(crossed == 0, FIRST[0], jnp.where(crossed == 1, FIRST[1], FIRST[2]))
+        entry = jnp.where(back == 0, HOME, first + d)
+        return jnp.where(other, 1, 0), entry
+
+    def matches(way, entry, side):
+        code = jnp.where(which_half == side, local_code + base, -2).astype(f32)
+        m = pool_meta[way, entry][:, 0:room]
+        return code == m[0:1, :], code == m[1:2, :], m
+
+    def pick_of(way, entry, side):
+        first_hit, second_hit, _ = matches(way, entry, side)
         return (first_hit | second_hit).astype(f32).astype(bf16)
 
-    def weights_of(slot, second):
-        first_hit, second_hit, m = matches(slot, second)
+    def weights_of(way, entry, side):
+        first_hit, second_hit, m = matches(way, entry, side)
         w = jnp.where(first_hit, m[2:3, :], 0.0) + jnp.where(second_hit, m[3:4, :], 0.0)
         high = w.astype(bf16)
         return high, (w - high.astype(f32)).astype(bf16)
@@ -298,12 +454,12 @@
         )
 
     def pick(step):
-        a, b = step, ring - 1 - step
-        one_a, one_b = pick_of(a, False), pick_of(b, True)
+        a, b = locate(step), locate(ring - 1 - step)
+        one_a, one_b = pick_of(*a, 0), pick_of(*b, 1)
         for c in range(width // tile):
             cols = pl.ds(c * tile, tile)
-            got = jnp.dot(one_a, pool[a, :, cols], preferred_element_type=f32)
-            got += jnp.dot(one_b, pool[b, :, cols], preferred_element_type=f32)
+            got = jnp.dot(one_a, pool[a[0], a[1], :, cols], preferred_element_type=f32)
+            got += jnp.dot(one_b, pool[b[0], b[1], :, cols], preferred_element_type=f32)
             got = got.astype(bf16).reshape(peers, 2 * CAP, tile)
             picked[step, :, :, cols] = got
         for o in range(1, peers):
@@ -325,48 +481,28 @@
             exchange(made, back, back_send, back_recv, step, o).start()
         back[step, mine] = made[step, mine]
 
-    def ring_step(n, _):
-        for h in range(2):
-            send_pool(0, n - 1, h).wait_recv()
-
-            @pl.when((n < far - 1) | (h == 0))
-            def _():
-                send_pool(0, n, h).start()
-
-            send_pool(1, lax.rem(ring - n + 1, ring), h).wait_recv()
-
-            @pl.when((n < far - 1) | (h == 1))
-            def _():
-                send_pool(1, ring - n, h).start()
-
-            if h == 0:
-                send_meta(0, n - 1).wait_recv()
-                send_meta(0, n).start()
-                send_meta(1, lax.rem(ring - n + 1, ring)).wait_recv()
-
-                @pl.when(n < far - 1)
-                def _():
-                    send_meta(1, ring - n).start()
-
-                @pl.when(n == 1)
-                def _():
-                    own_rows(1)
-
-                @pl.when(n >= 2)
-                def _():
-                    serve(n - 2)
-            else:
-                pick(n - 1)
+    def ring_step(d, _):
+        for kind in (2, 1, 0):
+            for way in range(2):
+                receive(way, kind, d)
+                forward(way, kind, d, start_both)
+
+        @pl.when(d <= far - 2)
+        def _():
+            pick(d - 1)
+
+        @pl.when((d >= 2) & (d <= far - 1))
+        def _():
+            serve(d - 2)
+
         return 0
 
     for load in loads[2:]:
         load.wait()
-    lax.fori_loop(1, far, ring_step, 0)
+    lax.fori_loop(1, LAST[2] + 1, ring_step, 0)
+    pick(far - 2)
+    pick(far - 1)
     serve(far - 2)
-    send_meta(0, far - 1).wait_recv()
-    send_pool(0, far - 1, 0).wait_recv()
-    send_pool(1, ring - far + 1, 1).wait_recv()
-    pick(far - 1)
     serve(far - 1)
 
     contract = (((0,), (0,)), ((), ()))
@@ -375,90 +511,147 @@
         for o in range(1, peers):
             exchange(made, back, back_send, back_recv, step, o).wait_recv()
 
-    def own_share(slot, step, second, dst):
-        high, low = weights_of(slot, second)
+    def own_share(way, entry, behind, dst):
+        side = jnp.where(behind >= far, 1, 0)
+        step = jnp.where(behind >= far, ring - 1 - behind, behind)
+        high, low = weights_of(way, entry, side)
         w = jnp.concatenate([high, low], axis=0)
         for c in range(width // tile):
             cols = pl.ds(c * tile, tile)
-            y = back[step, :, :, cols].reshape(peers * 2 * CAP, tile)
+            y = back[step, :, :, cols].reshape(room, tile)
             y = jnp.concatenate([y, y], axis=0)
             dst[:, cols] = lax.dot_general(w, y, contract, preferred_element_type=f32)
 
-    def send_sum(way, d, h):
-        buf = left_sum if way == 0 else right_sum
+    def send_sum(way, kind, d, count):
+        entry = FIRST[kind] + d
         return pltpu.make_async_remote_copy(
-            src_ref=buf.at[d, part(h)],
-            dst_ref=buf.at[d - 1, part(h)],
-            send_sem=sum_send.at[way, d - 1, h],
-            recv_sem=sum_recv.at[way, d - 1, h],
-            device_id=prv if way == 0 else nxt,
+            src_ref=sums.at[way, entry, pl.ds(0, count)],
+            dst_ref=sums.at[way, entry - 1, pl.ds(0, count)],
+            send_sem=sum_send.at[way, entry],
+            recv_sem=sum_recv.at[way, entry - 1],
+            device_id=onward[1 - way],
             device_id_type=MESH_ID,
         )
 
+    def give_back(way, kind, d, act):
+        goes = passes(way, kind, d)
+        short = is_mine(way, kind, d) & (ends[way] == SPAN - 1)
+
+        @pl.when(goes & ~short)
+        def _():
+            act(send_sum(way, kind, d, room))
+
+        @pl.when(goes & short)
+        def _():
+            act(send_sum(way, kind, d, room // 2))
+
+    first_rows, last_rows = pl.ds(0, room // 2), pl.ds(room // 2, room // 2)
+
+    def sum_entry(way, kind, d):
+        entry = FIRST[kind] + d
+        goes = passes(way, kind, d)
+        mine_here = is_mine(way, kind, d)
+        end = ends[way]
+
+        @pl.when(goes & (~mine_here | (end < SPAN - 2)))
+        def _():
+            send_sum(way, kind, d + 1, room).wait_recv()
+
+        @pl.when(goes & mine_here & (end < SPAN - 2))
+        def _():
+            sums[way, entry] = (sums[way, entry].astype(f32) + own_part[way]).astype(bf16)
+
+        @pl.when(goes & mine_here & (end == SPAN - 2))
+        def _():
+            sums[way, entry, last_rows] = own_part[way, last_rows].astype(bf16)
+            send_sum(way, kind, d + 1, room // 2).wait_recv()
+            got = sums[way, entry, first_rows].astype(f32) + own_part[way, first_rows]
+            sums[way, entry, first_rows] = got.astype(bf16)
+
+        @pl.when(goes & mine_here & (end == SPAN - 1))
+        def _():
+            sums[way, entry, first_rows] = own_part[way, first_rows].astype(bf16)
+
+        give_back(way, kind, d, lambda copy: copy.start())
+
     wait_back(far - 1)
-    own_share(far, far - 1, True, left_own)
-    left_sum[far, part(0)] = left_own[part(0)].astype(bf16)
-    send_sum(0, far, 0).start()
-    right_sum[far, part(1)] = left_own[part(1)].astype(bf16)
-    send_sum(1, far, 1).start()
+    wait_back(far - 2)
 
     def sum_step(i, _):
-        d = far - 1 - i
-        wait_back(d - 1)
-        own_share(d, d, False, left_own)
-        own_share(ring - d, d - 1, True, right_own)
-        for way, own, buf, order in ((0, left_own, left_sum, (1, 0)), (1, right_own, right_sum, (0, 1))):
-            h = order[0]
-
-            @pl.when(d < far - 1)
-            def _():
-                send_sum(way, d + 1, h).wait_recv()
-                buf[d, part(h)] = (buf[d, part(h)].astype(f32) + own[part(h)]).astype(bf16)
-
-            @pl.when(d == far - 1)
-            def _():
-                buf[d, part(h)] = own[part(h)].astype(bf16)
-
-            send_sum(way, d, h).start()
-        for way, own, buf, order in ((0, left_own, left_sum, (1, 0)), (1, right_own, right_sum, (0, 1))):
-            h = order[1]
-            send_sum(way, d + 1, h).wait_recv()
-            buf[d, part(h)] = (buf[d, part(h)].astype(f32) + own[part(h)]).astype(bf16)
-            send_sum(way, d, h).start()
+        d = LAST[2] - i
+
+        @pl.when(d <= far - 2)
+        def _():
+            wait_back(d - 1)
+
+        for kind in range(3):
+            for way in range(2):
+
+                @pl.when(passes(way, kind, d) & is_mine(way, kind, d))
+                def _():
+                    behind = d if way == 0 else ring - d
+                    own_share(way, FIRST[kind] + d, behind, own_part.at[way])
+
+        for kind in range(3):
+            for way in range(2):
+                sum_entry(way, kind, d)
         return 0
 
-    lax.fori_loop(0, far - 1, sum_step, 0)
-    own_share(0, 0, False, left_own)
-    left_own[...] += stream[...].astype(f32)
-    for h in (1, 0):
-        send_sum(0, 1, h).wait_recv()
-        send_sum(1, 1, h).wait_recv()
-        total = left_own[part(h)] + left_sum[0, part(h)].astype(f32)
-        out_ref[part(h)] = (total + right_sum[0, part(h)].astype(f32)).astype(bf16)
-
-    def drain(n, _):
-        for way in range(2):
-            slot = n if way == 0 else lax.rem(ring - n, ring)
-            for h in range(2):
-
-                @pl.when((n < far - 1) | (h == way))
+    lax.fori_loop(0, LAST[2], sum_step, 0)
+    own_share(0, HOME, 0, own_part.at[0])
+
+    def place(n, value):
+        choose = packing(n)
+        for c in range(width // tile):
+            cols = pl.ds(c * tile, tile)
+            got = lax.dot_general(choose, value(cols), contract, preferred_element_type=f32)
+            total[:, cols] += got
+
+    total[...] = stream[...].astype(f32)
+    place(5, lambda cols: own_part[0, :, cols].astype(bf16))
+
+    def land(n, way, kind):
+        whole, first = forwards(way, kind, 0)
+
+        @pl.when(whole)
+        def _():
+            send_sum(way, kind, 1, room).wait_recv()
+
+        @pl.when(first)
+        def _():
+            send_sum(way, kind, 1, room // 2).wait_recv()
+            sums[way, FIRST[kind], last_rows] = jnp.zeros((room // 2, width), bf16)
+
+        @pl.when(whole | first)
+        def _():
+            place(n, lambda cols: sums[way, FIRST[kind], :, cols])
+
+    for n, way, kind in ((0, 0, 0), (2, 1, 0), (1, 0, 1), (3, 1, 1)):
+        land(n, way, kind)
+    for way in range(2):
+        land(4, way, 2)
+    out_ref[...] = total[...].astype(bf16)
+
+    def drain(d, _):
+        for kind in range(3):
+            for way in range(2):
+                forward(way, kind, d, wait_sent)
+
+                @pl.when(d >= 1)
                 def _():
-                    send_pool(way, slot, h).wait_send()
-
-                @pl.when((n < far - 1) | (h == way))
-                def _():
-                    send_sum(way, n + 1, h).wait_send()
-
-            @pl.when((n < far - 1) | (way == 0))
-            def _():
-                send_meta(way, slot).wait_send()
-
+                    give_back(way, kind, d, lambda copy: copy.wait_send())
+
+        return 0
+
+    lax.fori_loop(0, LAST[2] + 1, drain, 0)
+
+    def drain_steps(n, _):
         for o in range(1, peers):
             exchange(picked, routed, pick_send, pick_recv, n, o).wait_send()
             exchange(made, back, back_send, back_recv, n, o).wait_send()
         return 0
 
-    lax.fori_loop(0, far, drain, 0)
+    lax.fori_loop(0, far, drain_steps, 0)
     halo.wait_send()
     for h in range(2):
         for way in range(2):
@@ -466,13 +659,14 @@
             send_near(way, h).wait_send()
 
 
-def layer(query, key, value, cosines, sines, sinks, gain, meta, residual, proj, gate, up, down):
+def layer(query, key, value, cosines, sines, sinks, gain, ids, mix, residual, proj, gate, up, down):
     rows, width = residual.shape
     ring = lax.axis_size("sp") // CORES
     xs = lax.axis_size("tp")
     far = ring // 2
     peers = xs * CORES
     hidden = gate.shape[1]
+    room = 2 * peers * CAP
     tile = min(512, width)
     bf16, f32 = jnp.bfloat16, jnp.float32
     vmem = pl.BlockSpec(memory_space=pltpu.VMEM)
@@ -483,7 +677,7 @@
     return pl.pallas_call(
         functools.partial(expert_kernel, ring, xs, tile),
         out_shape=jax.ShapeDtypeStruct((rows, width), bf16),
-        in_specs=[vmem] * 5 + [smem] + [vmem] * 2 + [hbm] * 5,
+        in_specs=[vmem] * 5 + [smem] + [vmem] * 3 + [hbm] * 5,
         out_specs=vmem,
         scratch_shapes=[
             pltpu.VMEM(query.shape, bf16),
@@ -495,30 +689,31 @@
             pltpu.VMEM((2, 2, rows // 2, width), bf16),
             pltpu.VMEM((rows, width), f32),
             pltpu.VMEM((rows, width), bf16),
-            pltpu.VMEM((ring, rows, width), bf16),
-            pltpu.VMEM((ring, 8, rows), f32),
+            pltpu.VMEM((rows, width), bf16),
+            pltpu.VMEM((8, rows), f32),
+            pltpu.VMEM((2, ENTRIES, room, width), bf16),
+            pltpu.VMEM((rows, width), f32),
+            pltpu.VMEM((2, ENTRIES + 1, room, width), bf16),
+            pltpu.VMEM((2, ENTRIES + 1, 8, rows), f32),
             pltpu.VMEM(slab, bf16),
             pltpu.VMEM(slab, bf16),
             pltpu.VMEM(slab, bf16),
             pltpu.VMEM(slab, bf16),
-            pltpu.VMEM((far + 1, rows, width), bf16),
-            pltpu.VMEM((far + 1, rows, width), bf16),
-            pltpu.VMEM((rows, width), f32),
-            pltpu.VMEM((rows, width), f32),
+            pltpu.VMEM((2, room, width), f32),
             pltpu.VMEM((width, hidden), bf16),
             pltpu.VMEM((width, hidden), bf16),
             pltpu.VMEM((hidden, width), bf16),
             dma((5,)),
-            dma((2, far, 2)),
-            dma((2, far, 2)),
-            dma((2, far)),
-            dma((2, far)),
+            dma((2, ENTRIES)),
+            dma((2, ENTRIES)),
+            dma((2, ENTRIES)),
+            dma((2, ENTRIES)),
             dma((far, peers)),
             dma((far, peers)),
             dma((far, peers)),
             dma((far, peers)),
-            dma((2, far, 2)),
-            dma((2, far, 2)),
+            dma((2, ENTRIES)),
+            dma((2, ENTRIES)),
             dma,
             dma,
             dma((2, 2)),
@@ -529,7 +724,7 @@
         compiler_params=pltpu.CompilerParams(
             collective_id=1, has_side_effects=True, vmem_limit_bytes=60 * 1024 * 1024
         ),
-    )(query, key, value, cosines, sines, sinks, gain, meta, residual, proj, gate, up, down)
+    )(query, key, value, cosines, sines, sinks, gain, ids, mix, residual, proj, gate, up, down)
 
 
 def per_device(
@@ -547,23 +742,12 @@
     route_weight,
 ):
     tok_count = query_rows.shape[0]
-    row_count = residual.shape[0]
     positions = lax.axis_index("sp") * tok_count + jnp.arange(tok_count, dtype=jnp.int32)
     half_dim = HDIM // 2
     inverse = rope_base ** (-jnp.arange(half_dim, dtype=jnp.float32) / half_dim)
     angles = positions.astype(jnp.float32)[:, None] * inverse[None, :]
     cosines = jnp.tile(jnp.cos(angles), (1, 128 // half_dim))
     sines = jnp.tile(jnp.sin(angles), (1, 128 // half_dim))
-    expert_count = lax.axis_size("sp") * lax.axis_size("tp")
-    flat_expert = routes.reshape(-1)
-    one_hot = (flat_expert[:, None] == jnp.arange(expert_count, dtype=jnp.int32)[None, :]).astype(
-        jnp.int32
-    )
-    slot_rank = jnp.sum((jnp.cumsum(one_hot, axis=0) - one_hot) * one_hot, axis=1)
-    codes = (flat_expert * CAP + slot_rank).astype(jnp.float32).reshape(row_count, 2)
-    meta = jnp.concatenate(
-        [codes.T, route_weight.T, jnp.zeros((4, row_count), jnp.float32)], axis=0
-    )
     return layer(
         query_rows,
         key_rows,
@@ -572,7 +756,8 @@
         sines,
         sink_logits,
         norm_gain[None, :],
-        meta,
+        routes.T,
+        route_weight.T,
         residual,
         out_weight,
         gate_weight[0],

time: 253 us -> 222 us (0.88)
  Pallas kernels: 241 us -> 214 us
    pallas_call x1, Pallas kernels: 241 us -> 214 us  [layer(): pl.pallas_call(functools.partial(expert_kernel, ring, xs, tile), out_shap...]
    unnamed x5 -> x3, local copies, waits for them, and re-layouts: 5.88 us -> 5.09 us
where the time goes in v3:
time: 222 us; the launch traced here: 221 us
  Pallas kernels  214 us (96%)
  local copies, waits for them, and re-layouts  6.79 us (3%)
    pallas_call x1, Pallas kernels, layer(): pl.pallas_call(functools.partial(expert_kernel, ring, xs, tile), out_shap...  214 us
    unnamed x3, local copies, waits for them, and re-layouts  5.09 us

profile of v3, /device:TPU:40, one launch (start us, length us, event | category | flops | bytes accessed | tf_op | source)
XLA Modules:
  0.0 221.2 jit_solution(12966925326831561285)
XLA Ops:
  0.0 0.3 multiply_sine_fusion
  0.3 1.6 copy.15.key_ref
  1.9 1.6 copy.16.value_ref
  3.6 0.8 copy.18.sin_ref
  4.4 0.8 copy.17.cos_ref
  5.3 214.1 %shard_map.118 = bf16[128,2048]{1,0:T(8,128)(2,1)} custom-call(bf16[512,256]{1,0:T(8,128)(2,1)} %query_ref.1, bf16[512,64]{1,0:T(8,128)(2,1)} %copy.15.key_ref, bf16[512,64]{1,0:T(8,128)(2,1)} %copy.16.value_ref, f32[512,128]{1,0:T(8,128)} %copy.17.cos_ref, f32[512,128]{1,0:T(8,128)} %copy.18.sin_ref, f32[4]{0:T(128)} %sink_ref.1, f32[1,2048]{1,0:T(1,128)} %bitcast.13, ...), custom_call_target="tpu_custom_call" | custom-call | tf_op jit(solution)/shard_map/pallas_call | solution.py:677
  219.3 1.9 copy.20
  (4 shorter events, 0.1 us)

commit v4 on v3

--- a/solution.py
+++ b/solution.py
@@ -137,21 +137,29 @@
         return (x.astype(f32) * cosines + swapped * sines).astype(bf16)
 
     tok = query_ref.shape[0]
-    keys_values[WINDOW:, 0:HDIM] = rotated(key_ref[...], cos_ref[:, 0:HDIM], sin_ref[:, 0:HDIM])
-    keys_values[WINDOW:, HDIM:] = value_ref[...]
+    k_low = key_ref[0 : HDIM // 2].astype(f32)
+    k_high = key_ref[HDIM // 2 :].astype(f32)
+    turned_low = k_low * cos_ref[...] - k_high * sin_ref[...]
+    turned_high = k_high * cos_ref[...] + k_low * sin_ref[...]
+    turned_k = jnp.concatenate([turned_low, turned_high], axis=0)
+    keys_values[0:HDIM, WINDOW:] = turned_k.astype(bf16)
+    keys_values[HDIM:, WINDOW:] = value_ref[...]
     pl.semaphore_wait(barrier, peers + 2)
     halo = pltpu.make_async_remote_copy(
-        src_ref=keys_values.at[pl.ds(tok, WINDOW)],
-        dst_ref=keys_values.at[pl.ds(0, WINDOW)],
+        src_ref=keys_values.at[:, pl.ds(tok, WINDOW)],
+        dst_ref=keys_values.at[:, pl.ds(0, WINDOW)],
         send_sem=halo_send,
         recv_sem=halo_recv,
         device_id=after,
         device_id_type=MESH_ID,
     )
     halo.start()
+    repeats = 128 // (HDIM // 2)
+    cosines = jnp.concatenate([cos_ref[...]] * repeats, axis=0).T
+    sines = jnp.concatenate([sin_ref[...]] * repeats, axis=0).T
     for c in range(query_ref.shape[1] // 128):
         cols = pl.ds(c * 128, 128)
-        rot_q[:, cols] = rotated(query_ref[:, cols], cos_ref[...], sin_ref[...])
+        rot_q[:, cols] = rotated(query_ref[:, cols], cosines, sines)
     halo.wait_recv()
 
     def part(h):
@@ -249,20 +257,21 @@
         start = pl.multiple_of(block * WINDOW, WINDOW)
         first = start + sp * tok
         allowed = (reach >= 0) & (reach < WINDOW) & (k_at + first >= WINDOW)
-        kv = keys_values[pl.ds(start, 2 * WINDOW), :]
-        k, v = kv[:, 0:HDIM], kv[:, HDIM:]
+        k = keys_values[0:HDIM, pl.ds(start, 2 * WINDOW)]
+        v = keys_values[HDIM:, pl.ds(start, 2 * WINDOW)]
         q = rot_q[pl.ds(start, WINDOW), :]
         heads = []
         for h in range(q.shape[1] // HDIM):
             qh = q[:, h * HDIM : (h + 1) * HDIM]
-            s = lax.dot_general(qh, k, (((1,), (1,)), ((), ())), preferred_element_type=f32)
+            s = jnp.dot(qh, k, preferred_element_type=f32)
             s = jnp.where(allowed, s * HDIM ** (-0.5), -jnp.inf)
             sink = sink_ref[h]
             top = jnp.maximum(jnp.max(s, axis=1, keepdims=True), sink)
             e = jnp.exp(s - top)
             below = jnp.sum(e, axis=1, keepdims=True) + jnp.exp(sink - top)
             p = (e / below).astype(bf16)
-            heads.append(jnp.dot(p, v, preferred_element_type=f32).astype(bf16))
+            seen = lax.dot_general(p, v, (((1,), (1,)), ((), ())), preferred_element_type=f32)
+            heads.append(seen.astype(bf16))
         att = jnp.concatenate(heads, axis=1)
         for c in range(width // tile):
             cols = pl.ds(c * tile, tile)
@@ -500,11 +509,6 @@
     for load in loads[2:]:
         load.wait()
     lax.fori_loop(1, LAST[2] + 1, ring_step, 0)
-    pick(far - 2)
-    pick(far - 1)
-    serve(far - 2)
-    serve(far - 1)
-
     contract = (((0,), (0,)), ((), ()))
 
     def wait_back(step):
@@ -574,17 +578,8 @@
 
         give_back(way, kind, d, lambda copy: copy.start())
 
-    wait_back(far - 1)
-    wait_back(far - 2)
-
-    def sum_step(i, _):
-        d = LAST[2] - i
-
-        @pl.when(d <= far - 2)
-        def _():
-            wait_back(d - 1)
-
-        for kind in range(3):
+    def return_kinds(kinds, d):
+        for kind in kinds:
             for way in range(2):
 
                 @pl.when(passes(way, kind, d) & is_mine(way, kind, d))
@@ -592,13 +587,9 @@
                     behind = d if way == 0 else ring - d
                     own_share(way, FIRST[kind] + d, behind, own_part.at[way])
 
-        for kind in range(3):
+        for kind in kinds:
             for way in range(2):
                 sum_entry(way, kind, d)
-        return 0
-
-    lax.fori_loop(0, LAST[2], sum_step, 0)
-    own_share(0, HOME, 0, own_part.at[0])
 
     def place(n, value):
         choose = packing(n)
@@ -607,26 +598,60 @@
             got = lax.dot_general(choose, value(cols), contract, preferred_element_type=f32)
             total[:, cols] += got
 
+    def land(n, way, kind):
+        whole, first = forwards(way, kind, 0)
+
+        @pl.when(whole)
+        def _():
+            send_sum(way, kind, 1, room).wait_recv()
+
+        @pl.when(first)
+        def _():
+            send_sum(way, kind, 1, room // 2).wait_recv()
+            sums[way, FIRST[kind], last_rows] = jnp.zeros((room // 2, width), bf16)
+
+        @pl.when(whole | first)
+        def _():
+            place(n, lambda cols: sums[way, FIRST[kind], :, cols])
+
+    pick(far - 2)
+    pick(far - 1)
+    wait_back(3)
+    wait_back(2)
+    return_kinds((0,), 3)
+    serve(far - 2)
+    wait_back(1)
+    return_kinds((0,), 2)
+    serve(far - 1)
+    wait_back(0)
+    return_kinds((0,), 1)
+    own_share(0, HOME, 0, own_part.at[0])
     total[...] = stream[...].astype(f32)
     place(5, lambda cols: own_part[0, :, cols].astype(bf16))
-
-    def land(n, way, kind):
-        whole, first = forwards(way, kind, 0)
-
-        @pl.when(whole)
-        def _():
-            send_sum(way, kind, 1, room).wait_recv()
-
-        @pl.when(first)
-        def _():
-            send_sum(way, kind, 1, room // 2).wait_recv()
-            sums[way, FIRST[kind], last_rows] = jnp.zeros((room // 2, width), bf16)
-
-        @pl.when(whole | first)
-        def _():
-            place(n, lambda cols: sums[way, FIRST[kind], :, cols])
-
-    for n, way, kind in ((0, 0, 0), (2, 1, 0), (1, 0, 1), (3, 1, 1)):
+    wait_back(far - 1)
+    wait_back(far - 2)
+
+    def sum_step(i, _):
+        d = LAST[2] - i
+
+        @pl.when((d <= far - 2) & (d >= 5))
+        def _():
+            wait_back(d - 1)
+
+        return_kinds((1, 2), d)
+
+        @pl.when(d == 4)
+        def _():
+            land(0, 0, 0)
+
+        @pl.when(d == 3)
+        def _():
+            land(2, 1, 0)
+
+        return 0
+
+    lax.fori_loop(0, LAST[2], sum_step, 0)
+    for n, way, kind in ((1, 0, 1), (3, 1, 1)):
         land(n, way, kind)
     for way in range(2):
         land(4, way, 2)
@@ -681,7 +706,7 @@
         out_specs=vmem,
         scratch_shapes=[
             pltpu.VMEM(query.shape, bf16),
-            pltpu.VMEM((query.shape[0] + WINDOW, 2 * HDIM), bf16),
+            pltpu.VMEM((2 * HDIM, query.shape[0] + WINDOW), bf16),
             pltpu.VMEM((rows, width), bf16),
             pltpu.VMEM(proj.shape, bf16),
             pltpu.VMEM((3, rows, width), bf16),
@@ -745,13 +770,13 @@
     positions = lax.axis_index("sp") * tok_count + jnp.arange(tok_count, dtype=jnp.int32)
     half_dim = HDIM // 2
     inverse = rope_base ** (-jnp.arange(half_dim, dtype=jnp.float32) / half_dim)
-    angles = positions.astype(jnp.float32)[:, None] * inverse[None, :]
-    cosines = jnp.tile(jnp.cos(angles), (1, 128 // half_dim))
-    sines = jnp.tile(jnp.sin(angles), (1, 128 // half_dim))
+    angles = positions.astype(jnp.float32)[None, :] * inverse[:, None]
+    cosines = jnp.cos(angles)
+    sines = jnp.sin(angles)
     return layer(
         query_rows,
-        key_rows,
-        value_rows,
+        key_rows.T,
+        value_rows.T,
         cosines,
         sines,
         sink_logits,

time: 222 us -> 216 us (0.973)
  local copies, waits for them, and re-layouts: 6.79 us -> 1.88 us
    unnamed x3 -> x1, local copies, waits for them, and re-layouts: 5.09 us -> 1.88 us
    pallas_call x1, Pallas kernels: 214 us -> 212 us  [layer(): pl.pallas_call(functools.partial(expert_kernel, ring, xs, tile), out_shap...]
where the time goes in v4:
time: 216 us; the launch traced here: 215 us
  Pallas kernels  212 us (98%)
    pallas_call x1, Pallas kernels, layer(): pl.pallas_call(functools.partial(expert_kernel, ring, xs, tile), out_shap...  212 us

profile of v4, /device:TPU:40, one launch (start us, length us, event | category | flops | bytes accessed | tf_op | source)
XLA Modules:
  0.0 214.6 jit_solution(8362958532075423205)
XLA Ops:
  0.0 1.0 multiply_sine_fusion
  1.0 211.7 %shard_map.118 = bf16[128,2048]{1,0:T(8,128)(2,1)} custom-call(bf16[512,256]{1,0:T(8,128)(2,1)} %query_ref.1, bf16[64,512]{1,0:T(8,128)(2,1)} %bitcast.11, bf16[64,512]{1,0:T(8,128)(2,1)} %bitcast.12, f32[32,512]{1,0:T(8,128)} %get-tuple-element.6.cos_ref, f32[32,512]{1,0:T(8,128)} %get-tuple-element.5.sin_ref, f32[4]{0:T(128)} %sink_ref.1, ...), custom_call_target="tpu_custom_call" | custom-call | tf_op jit(solution)/shard_map/pallas_call | solution.py:702
  212.7 1.9 copy.14
  (2 shorter events, 0.0 us)

commit v5 on v4

--- a/solution.py
+++ b/solution.py
@@ -122,6 +122,28 @@
     after = {"sp": lax.rem(sp + 1, total_sp)}
     across = {"sp": lax.rem(sp + jnp.where(core == 1, 1, total_sp - 1), total_sp)}
     pl.semaphore_signal(barrier, inc=1, device_id=across, device_id_type=MESH_ID)
+    block, at = z // SPAN, lax.rem(z, SPAN)
+    opposite_way = jnp.where(at >= SPAN // 2, 0, 1)
+    ends = (at, SPAN - 1 - at)
+
+    def chips_on(count):
+        return {"sp": lax.rem(sp + (count + ring) * CORES, total_sp)}
+
+    def greet(count):
+        pl.semaphore_signal(barrier, inc=1, device_id=chips_on(count), device_id_type=MESH_ID)
+
+    greet(SPAN - ends[0])
+    greet(ends[1] - SPAN)
+    greet(jnp.where(opposite_way == 0, 2 * SPAN - ends[0], ends[1] - 2 * SPAN))
+    for way in range(2):
+
+        @pl.when(ends[way] == 0)
+        def _():
+            for d in range(1, SPAN + SPAN // 2 + 1):
+                greet(d if way else -d)
+
+    edge = (ends[0] == 0) | (ends[1] == 0)
+    greetings = peers + 2 + 3 + jnp.where(edge, SPAN + SPAN // 2, 0)
     for o in range(1, peers):
         pl.semaphore_signal(barrier, inc=1, device_id=peer(o)[1], device_id_type=MESH_ID)
 
@@ -144,7 +166,7 @@
     turned_k = jnp.concatenate([turned_low, turned_high], axis=0)
     keys_values[0:HDIM, WINDOW:] = turned_k.astype(bf16)
     keys_values[HDIM:, WINDOW:] = value_ref[...]
-    pl.semaphore_wait(barrier, peers + 2)
+    pl.semaphore_wait(barrier, greetings)
     halo = pltpu.make_async_remote_copy(
         src_ref=keys_values.at[:, pl.ds(tok, WINDOW)],
         dst_ref=keys_values.at[:, pl.ds(0, WINDOW)],
@@ -165,9 +187,6 @@
     def part(h):
         return pl.ds(h * half, half)
 
-    block, at = z // SPAN, lax.rem(z, SPAN)
-    opposite_way = jnp.where(at >= SPAN // 2, 0, 1)
-    ends = (at, SPAN - 1 - at)
     onward = (nxt, prv)
     room = 2 * peers * CAP
 
@@ -526,53 +545,55 @@
             y = jnp.concatenate([y, y], axis=0)
             dst[:, cols] = lax.dot_general(w, y, contract, preferred_element_type=f32)
 
-    def send_sum(way, kind, d, count):
+    def send_sum(way, kind, d, count, home=False):
         entry = FIRST[kind] + d
         return pltpu.make_async_remote_copy(
             src_ref=sums.at[way, entry, pl.ds(0, count)],
-            dst_ref=sums.at[way, entry - 1, pl.ds(0, count)],
+            dst_ref=sums.at[way, FIRST[kind] if home else entry - 1, pl.ds(0, count)],
             send_sem=sum_send.at[way, entry],
-            recv_sem=sum_recv.at[way, entry - 1],
-            device_id=onward[1 - way],
+            recv_sem=sum_recv.at[way, FIRST[kind] if home else entry - 1],
+            device_id=chips_on(d if way else -d) if home else onward[1 - way],
             device_id_type=MESH_ID,
         )
 
     def give_back(way, kind, d, act):
-        goes = passes(way, kind, d)
-        short = is_mine(way, kind, d) & (ends[way] == SPAN - 1)
-
-        @pl.when(goes & ~short)
+        goes = passes(way, kind, d) & is_mine(way, kind, d)
+        end = ends[way]
+
+        @pl.when(goes & (end == SPAN - 1))
+        def _():
+            act(send_sum(way, kind, d, room // 2))
+
+        @pl.when(goes & (end < SPAN - 1) & (end > 0))
         def _():
             act(send_sum(way, kind, d, room))
 
-        @pl.when(goes & short)
-        def _():
-            act(send_sum(way, kind, d, room // 2))
+        if kind > 0:
+
+            @pl.when(goes & (end == 0))
+            def _():
+                act(send_sum(way, kind, d, room, home=True))
 
     first_rows, last_rows = pl.ds(0, room // 2), pl.ds(room // 2, room // 2)
 
     def sum_entry(way, kind, d):
         entry = FIRST[kind] + d
-        goes = passes(way, kind, d)
-        mine_here = is_mine(way, kind, d)
+        goes = passes(way, kind, d) & is_mine(way, kind, d)
         end = ends[way]
 
-        @pl.when(goes & (~mine_here | (end < SPAN - 2)))
+        @pl.when(goes & (end < SPAN - 2))
         def _():
             send_sum(way, kind, d + 1, room).wait_recv()
-
-        @pl.when(goes & mine_here & (end < SPAN - 2))
-        def _():
             sums[way, entry] = (sums[way, entry].astype(f32) + own_part[way]).astype(bf16)
 
-        @pl.when(goes & mine_here & (end == SPAN - 2))
+        @pl.when(goes & (end == SPAN - 2))
         def _():
             sums[way, entry, last_rows] = own_part[way, last_rows].astype(bf16)
             send_sum(way, kind, d + 1, room // 2).wait_recv()
             got = sums[way, entry, first_rows].astype(f32) + own_part[way, first_rows]
             sums[way, entry, first_rows] = got.astype(bf16)
 
-        @pl.when(goes & mine_here & (end == SPAN - 1))
+        @pl.when(goes & (end == SPAN - 1))
         def _():
             sums[way, entry, first_rows] = own_part[way, first_rows].astype(bf16)
 

time: 216 us -> 229 us (1.060)
  Pallas kernels: 212 us -> 223 us
    pallas_call x1, Pallas kernels: 212 us -> 223 us  [layer(): pl.pallas_call(functools.partial(expert_kernel, ring, xs, tile), out_shap...]
where the time goes in v5:
time: 229 us; the launch traced here: 226 us
  Pallas kernels  223 us (97%)
    pallas_call x1, Pallas kernels, layer(): pl.pallas_call(functools.partial(expert_kernel, ring, xs, tile), out_shap...  223 us

profile of v5, /device:TPU:40, one launch (start us, length us, event | category | flops | bytes accessed | tf_op | source)
XLA Modules:
  0.0 225.8 jit_solution(364302023662282205)
XLA Ops:
  0.0 1.0 multiply_sine_fusion
  1.0 222.9 %shard_map.118 = bf16[128,2048]{1,0:T(8,128)(2,1)} custom-call(bf16[512,256]{1,0:T(8,128)(2,1)} %query_ref.1, bf16[64,512]{1,0:T(8,128)(2,1)} %bitcast.11, bf16[64,512]{1,0:T(8,128)(2,1)} %bitcast.12, f32[32,512]{1,0:T(8,128)} %get-tuple-element.6.cos_ref, f32[32,512]{1,0:T(8,128)} %get-tuple-element.5.sin_ref, f32[4]{0:T(128)} %sink_ref.1, ...), custom_call_target="tpu_custom_call" | custom-call | tf_op jit(solution)/shard_map/pallas_call | solution.py:723
  223.9 1.9 copy.14
  (2 shorter events, 0.0 us)

commit v6 on v4

--- a/solution.py
+++ b/solution.py
@@ -426,6 +426,10 @@
     which_half = lax.rem(row_id, 2 * CAP) // CAP
     base = z * (peers * CAP)
 
+    def paired(back):
+        late = (at == SPAN - 1) & ((back == far - 1) | (back == far + 1))
+        return jnp.where(late, ring - back, back)
+
     def locate(back):
         other = back > at + SPAN + SPAN // 2
         d = jnp.where(other, ring - back, back)
@@ -463,7 +467,7 @@
         )
 
     def pick(step):
-        a, b = locate(step), locate(ring - 1 - step)
+        a, b = locate(paired(step)), locate(paired(ring - 1 - step))
         one_a, one_b = pick_of(*a, 0), pick_of(*b, 1)
         for c in range(width // tile):
             cols = pl.ds(c * tile, tile)
@@ -496,11 +500,11 @@
                 receive(way, kind, d)
                 forward(way, kind, d, start_both)
 
-        @pl.when(d <= far - 2)
+        @pl.when(d <= far - 1)
         def _():
             pick(d - 1)
 
-        @pl.when((d >= 2) & (d <= far - 1))
+        @pl.when((d >= 2) & (d <= far))
         def _():
             serve(d - 2)
 
@@ -516,8 +520,9 @@
             exchange(made, back, back_send, back_recv, step, o).wait_recv()
 
     def own_share(way, entry, behind, dst):
-        side = jnp.where(behind >= far, 1, 0)
-        step = jnp.where(behind >= far, ring - 1 - behind, behind)
+        place_of = paired(behind)
+        side = jnp.where(place_of >= far, 1, 0)
+        step = jnp.where(place_of >= far, ring - 1 - place_of, place_of)
         high, low = weights_of(way, entry, side)
         w = jnp.concatenate([high, low], axis=0)
         for c in range(width // tile):
@@ -526,70 +531,65 @@
             y = jnp.concatenate([y, y], axis=0)
             dst[:, cols] = lax.dot_general(w, y, contract, preferred_element_type=f32)
 
-    def send_sum(way, kind, d, count):
+    def lines(h):
+        return pl.ds(h * (room // 2), room // 2)
+
+    def send_sum(way, kind, d, h):
         entry = FIRST[kind] + d
         return pltpu.make_async_remote_copy(
-            src_ref=sums.at[way, entry, pl.ds(0, count)],
-            dst_ref=sums.at[way, entry - 1, pl.ds(0, count)],
-            send_sem=sum_send.at[way, entry],
-            recv_sem=sum_recv.at[way, entry - 1],
+            src_ref=sums.at[way, entry, lines(h)],
+            dst_ref=sums.at[way, entry - 1, lines(h)],
+            send_sem=sum_send.at[way, entry, h],
+            recv_sem=sum_recv.at[way, entry - 1, h],
             device_id=onward[1 - way],
             device_id_type=MESH_ID,
         )
 
+    def gives(way, kind, d, h):
+        goes = passes(way, kind, d)
+        return goes if h == 0 else goes & ~(is_mine(way, kind, d) & (ends[way] == SPAN - 1))
+
     def give_back(way, kind, d, act):
-        goes = passes(way, kind, d)
-        short = is_mine(way, kind, d) & (ends[way] == SPAN - 1)
-
-        @pl.when(goes & ~short)
-        def _():
-            act(send_sum(way, kind, d, room))
-
-        @pl.when(goes & short)
-        def _():
-            act(send_sum(way, kind, d, room // 2))
-
-    first_rows, last_rows = pl.ds(0, room // 2), pl.ds(room // 2, room // 2)
-
-    def sum_entry(way, kind, d):
+        for h in range(2):
+
+            @pl.when(gives(way, kind, d, h))
+            def _():
+                act(send_sum(way, kind, d, h))
+
+    def sum_entry(way, kind, d, h):
         entry = FIRST[kind] + d
         goes = passes(way, kind, d)
         mine_here = is_mine(way, kind, d)
-        end = ends[way]
-
-        @pl.when(goes & (~mine_here | (end < SPAN - 2)))
-        def _():
-            send_sum(way, kind, d + 1, room).wait_recv()
-
-        @pl.when(goes & mine_here & (end < SPAN - 2))
-        def _():
-            sums[way, entry] = (sums[way, entry].astype(f32) + own_part[way]).astype(bf16)
-
-        @pl.when(goes & mine_here & (end == SPAN - 2))
-        def _():
-            sums[way, entry, last_rows] = own_part[way, last_rows].astype(bf16)
-            send_sum(way, kind, d + 1, room // 2).wait_recv()
-            got = sums[way, entry, first_rows].astype(f32) + own_part[way, first_rows]
-            sums[way, entry, first_rows] = got.astype(bf16)
-
-        @pl.when(goes & mine_here & (end == SPAN - 1))
-        def _():
-            sums[way, entry, first_rows] = own_part[way, first_rows].astype(bf16)
-
-        give_back(way, kind, d, lambda copy: copy.start())
-
-    def return_kinds(kinds, d):
-        for kind in kinds:
+        comes = ends[way] < SPAN - 1 - h
+
+        @pl.when(goes & (comes | ~mine_here))
+        def _():
+            send_sum(way, kind, d + 1, h).wait_recv()
+
+        @pl.when(goes & comes & mine_here)
+        def _():
+            got = sums[way, entry, lines(h)].astype(f32) + own_part[way, lines(h)]
+            sums[way, entry, lines(h)] = got.astype(bf16)
+
+        @pl.when(goes & ~comes & mine_here)
+        def _():
+            sums[way, entry, lines(h)] = own_part[way, lines(h)].astype(bf16)
+
+        @pl.when(gives(way, kind, d, h))
+        def _():
+            send_sum(way, kind, d, h).start()
+
+    def return_kind(kind, d):
+        for way in range(2):
+
+            @pl.when(passes(way, kind, d) & is_mine(way, kind, d))
+            def _():
+                behind = d if way == 0 else ring - d
+                own_share(way, FIRST[kind] + d, behind, own_part.at[way])
+
+        for h in (1, 0):
             for way in range(2):
-
-                @pl.when(passes(way, kind, d) & is_mine(way, kind, d))
-                def _():
-                    behind = d if way == 0 else ring - d
-                    own_share(way, FIRST[kind] + d, behind, own_part.at[way])
-
-        for kind in kinds:
-            for way in range(2):
-                sum_entry(way, kind, d)
+                sum_entry(way, kind, d, h)
 
     def place(n, value):
         choose = packing(n)
@@ -601,60 +601,53 @@
     def land(n, way, kind):
         whole, first = forwards(way, kind, 0)
 
+        @pl.when(whole | first)
+        def _():
+            send_sum(way, kind, 1, 0).wait_recv()
+
         @pl.when(whole)
         def _():
-            send_sum(way, kind, 1, room).wait_recv()
+            send_sum(way, kind, 1, 1).wait_recv()
 
         @pl.when(first)
         def _():
-            send_sum(way, kind, 1, room // 2).wait_recv()
-            sums[way, FIRST[kind], last_rows] = jnp.zeros((room // 2, width), bf16)
+            sums[way, FIRST[kind], lines(1)] = jnp.zeros((room // 2, width), bf16)
 
         @pl.when(whole | first)
         def _():
             place(n, lambda cols: sums[way, FIRST[kind], :, cols])
 
-    pick(far - 2)
     pick(far - 1)
-    wait_back(3)
-    wait_back(2)
-    return_kinds((0,), 3)
-    serve(far - 2)
-    wait_back(1)
-    return_kinds((0,), 2)
-    serve(far - 1)
     wait_back(0)
-    return_kinds((0,), 1)
     own_share(0, HOME, 0, own_part.at[0])
     total[...] = stream[...].astype(f32)
     place(5, lambda cols: own_part[0, :, cols].astype(bf16))
+    serve(far - 1)
+    wait_back(far - 2)
     wait_back(far - 1)
-    wait_back(far - 2)
 
     def sum_step(i, _):
-        d = LAST[2] - i
-
-        @pl.when((d <= far - 2) & (d >= 5))
-        def _():
-            wait_back(d - 1)
-
-        return_kinds((1, 2), d)
-
-        @pl.when(d == 4)
-        def _():
-            land(0, 0, 0)
-
-        @pl.when(d == 3)
-        def _():
-            land(2, 1, 0)
+        r = LAST[2] - 1 - i
+
+        @pl.when((r <= far - 2) & (r >= 2))
+        def _():
+            wait_back(r - 1)
+
+        @pl.when(r >= 1)
+        def _():
+            return_kind(1, r)
+
+        return_kind(2, r + 1)
+
+        @pl.when(r >= 1)
+        def _():
+            return_kind(0, r)
 
         return 0
 
     lax.fori_loop(0, LAST[2], sum_step, 0)
-    for n, way, kind in ((1, 0, 1), (3, 1, 1)):
+    for n, way, kind in ((1, 0, 1), (3, 1, 1), (0, 0, 0), (2, 1, 0), (4, 0, 2), (4, 1, 2)):
         land(n, way, kind)
-    for way in range(2):
-        land(4, way, 2)
     out_ref[...] = total[...].astype(bf16)
 
     def drain(d, _):
@@ -737,8 +730,8 @@
             dma((far, peers)),
             dma((far, peers)),
             dma((far, peers)),
-            dma((2, ENTRIES)),
-            dma((2, ENTRIES)),
+            dma((2, ENTRIES, 2)),
+            dma((2, ENTRIES, 2)),
             dma,
             dma,
             dma((2, 2)),

time: 216 us -> 212 us (0.981)
  Pallas kernels: 212 us -> 209 us
    pallas_call x1, Pallas kernels: 212 us -> 209 us  [layer(): pl.pallas_call(functools.partial(expert_kernel, ring, xs, tile), out_shap...]
where the time goes in v6:
time: 212 us
  Pallas kernels  209 us (99%)
    pallas_call x1, Pallas kernels, layer(): pl.pallas_call(functools.partial(expert_kernel, ring, xs, tile), out_shap...  209 us

profile of v6, /device:TPU:40, one launch (start us, length us, event | category | flops | bytes accessed | tf_op | source)
XLA Modules:
  0.0 212.0 jit_solution(1168350764602235802)
XLA Ops:
  0.0 1.0 multiply_sine_fusion
  1.0 209.1 %shard_map.118 = bf16[128,2048]{1,0:T(8,128)(2,1)} custom-call(bf16[512,256]{1,0:T(8,128)(2,1)} %query_ref.1, bf16[64,512]{1,0:T(8,128)(2,1)} %bitcast.11, bf16[64,512]{1,0:T(8,128)(2,1)} %bitcast.12, f32[32,512]{1,0:T(8,128)} %get-tuple-element.6.cos_ref, f32[32,512]{1,0:T(8,128)} %get-tuple-element.5.sin_ref, f32[4]{0:T(128)} %sink_ref.1, ...), custom_call_target="tpu_custom_call" | custom-call | tf_op jit(solution)/shard_map/pallas_call | solution.py:695
  210.1 1.9 copy.14
  (2 shorter events, 0.0 us)

commit v7 on v6

--- a/solution.py
+++ b/solution.py
@@ -622,30 +622,34 @@
     own_share(0, HOME, 0, own_part.at[0])
     total[...] = stream[...].astype(f32)
     place(5, lambda cols: own_part[0, :, cols].astype(bf16))
+    wait_back(far - 2)
+    return_kind(1, LAST[1])
     serve(far - 1)
-    wait_back(far - 2)
-    wait_back(far - 1)
 
     def sum_step(i, _):
-        r = LAST[2] - 1 - i
-
-        @pl.when((r <= far - 2) & (r >= 2))
-        def _():
-            wait_back(r - 1)
-
-        @pl.when(r >= 1)
-        def _():
-            return_kind(1, r)
+        r = far - i
+
+        @pl.when((r >= 4) & (r <= far))
+        def _():
+            wait_back(r - 3)
+
+        @pl.when(r == jnp.where((at == 0) | (at == SPAN - 1), far, far - 1))
+        def _():
+            wait_back(far - 1)
 
         return_kind(2, r + 1)
 
-        @pl.when(r >= 1)
+        @pl.when((r >= 1) & (r <= LAST[0]))
         def _():
             return_kind(0, r)
 
+        @pl.when(r >= 3)
+        def _():
+            return_kind(1, r - 2)
+
         return 0
 
-    lax.fori_loop(0, LAST[2], sum_step, 0)
+    lax.fori_loop(0, far + 1, sum_step, 0)
     for n, way, kind in ((1, 0, 1), (3, 1, 1), (0, 0, 0), (2, 1, 0), (4, 0, 2), (4, 1, 2)):
         land(n, way, kind)
     out_ref[...] = total[...].astype(bf16)

time: 212 us -> 212 us (level)
  no operation moved by 1% of the time
where the time goes in v7:
time: 212 us
  Pallas kernels  209 us (99%)
    pallas_call x1, Pallas kernels, layer(): pl.pallas_call(functools.partial(expert_kernel, ring, xs, tile), out_shap...  209 us

profile of v7, /device:TPU:40, one launch (start us, length us, event | category | flops | bytes accessed | tf_op | source)
XLA Modules:
  0.0 212.2 jit_solution(1482100234147634984)
XLA Ops:
  0.0 1.0 multiply_sine_fusion
  1.0 209.3 %shard_map.118 = bf16[128,2048]{1,0:T(8,128)(2,1)} custom-call(bf16[512,256]{1,0:T(8,128)(2,1)} %query_ref.1, bf16[64,512]{1,0:T(8,128)(2,1)} %bitcast.11, bf16[64,512]{1,0:T(8,128)(2,1)} %bitcast.12, f32[32,512]{1,0:T(8,128)} %get-tuple-element.6.cos_ref, f32[32,512]{1,0:T(8,128)} %get-tuple-element.5.sin_ref, f32[4]{0:T(128)} %sink_ref.1, ...), custom_call_target="tpu_custom_call" | custom-call | tf_op jit(solution)/shard_map/pallas_call | solution.py:699
  210.3 1.9 copy.14
  (2 shorter events, 0.0 us)

commit v8 on v7

--- a/solution.py
+++ b/solution.py
@@ -52,7 +52,7 @@
     near_in,
     own_share_sum,
     stream,
-    normed,
+    unscaled,
     places,
     sums,
     total,
@@ -165,6 +165,9 @@
     def part(h):
         return pl.ds(h * half, half)
 
+    def side_cols(h):
+        return pl.ds(h * (width // 2), width // 2)
+
     block, at = z // SPAN, lax.rem(z, SPAN)
     opposite_way = jnp.where(at >= SPAN // 2, 0, 1)
     ends = (at, SPAN - 1 - at)
@@ -183,13 +186,13 @@
     def is_mine(way, kind, d):
         return origin(way, d)[1] == kind
 
-    def send_chunk(way, kind, d, count):
+    def send_chunk(way, kind, d, count, h):
         entry = FIRST[kind] + d
         return pltpu.make_async_remote_copy(
-            src_ref=pool.at[way, entry, pl.ds(0, count)],
-            dst_ref=pool.at[way, entry + 1, pl.ds(0, count)],
-            send_sem=pool_send.at[way, entry],
-            recv_sem=pool_recv.at[way, entry + 1],
+            src_ref=pool.at[way, entry, pl.ds(0, count), side_cols(h)],
+            dst_ref=pool.at[way, entry + 1, pl.ds(0, count), side_cols(h)],
+            send_sem=pool_send.at[way, entry, h],
+            recv_sem=pool_recv.at[way, entry + 1, h],
             device_id=onward[way],
             device_id_type=MESH_ID,
         )
@@ -211,43 +214,52 @@
         whole = goes & jnp.where(mine_here, ends[way] < SPAN - 2, True)
         return whole, goes & mine_here & (ends[way] == SPAN - 2)
 
-    def forward(way, kind, d, act):
+    def forward(way, kind, d, h, act):
         whole, first = forwards(way, kind, d)
 
         @pl.when(whole)
         def _():
-            act(send_chunk(way, kind, d, room), send_meta(way, kind, d))
+            act(send_chunk(way, kind, d, room, h))
 
         @pl.when(first)
         def _():
-            act(send_chunk(way, kind, d, room // 2), send_meta(way, kind, d))
-
-    def start_both(chunk, about):
-        about.start()
-        chunk.start()
-
-    def wait_sent(chunk, about):
-        about.wait_send()
-        chunk.wait_send()
-
-    def receive(way, kind, d):
+            act(send_chunk(way, kind, d, room // 2, h))
+
+        if h == 1:
+
+            @pl.when(whole | first)
+            def _():
+                act(send_meta(way, kind, d))
+
+    def begin(copy):
+        copy.start()
+
+    def finish(copy):
+        copy.wait_send()
+
+    def receive(way, kind, d, h):
         goes = passes(way, kind, d)
         short = is_mine(way, kind, d) & (ends[way] == SPAN - 1)
 
-        @pl.when(goes)
-        def _():
-            send_meta(way, kind, d - 1).wait_recv()
-
         @pl.when(goes & ~short)
         def _():
-            send_chunk(way, kind, d - 1, room).wait_recv()
+            send_chunk(way, kind, d - 1, room, h).wait_recv()
 
         @pl.when(goes & short)
         def _():
-            send_chunk(way, kind, d - 1, room // 2).wait_recv()
-            pool[way, FIRST[kind] + d, pl.ds(room // 2, room // 2)] = jnp.zeros(
-                (room // 2, width), bf16
-            )
+            send_chunk(way, kind, d - 1, room // 2, h).wait_recv()
+
+        if h == 1:
+
+            @pl.when(goes)
+            def _():
+                send_meta(way, kind, d - 1).wait_recv()
+
+            @pl.when(goes & short)
+            def _():
+                pool[way, FIRST[kind] + d, pl.ds(room // 2, room // 2)] = jnp.zeros(
+                    (room // 2, width), bf16
+                )
 
     q_at = lax.broadcasted_iota(jnp.int32, (WINDOW, 2 * WINDOW), 0)
     k_at = lax.broadcasted_iota(jnp.int32, (WINDOW, 2 * WINDOW), 1)
@@ -280,12 +292,9 @@
     def beside(step):
         return {"tp": lax.rem(tp + step + xs, xs)}
 
-    quarter = half // 2
-
     def send_far(way, h):
-        at = h * half + way * quarter
         return pltpu.make_async_remote_copy(
-            src_ref=shares.at[2, pl.ds(at, quarter)],
+            src_ref=shares.at[2, part(way), side_cols(h)],
             dst_ref=far_in.at[way, h],
             send_sem=far_send.at[way, h],
             recv_sem=far_recv.at[way, h],
@@ -295,7 +304,7 @@
 
     def send_near(way, h):
         return pltpu.make_async_remote_copy(
-            src_ref=shares.at[way, part(h)],
+            src_ref=shares.at[way, :, side_cols(h)],
             dst_ref=near_in.at[way, h],
             send_sem=near_send.at[way, h],
             recv_sem=near_recv.at[way, h],
@@ -314,26 +323,22 @@
             own_share_sum[:, cols] = y
         for h in range(2):
             send_far(way, h).wait_recv()
-            joint = pl.ds(h * half + way * quarter, quarter)
-            alone = pl.ds(h * half + (1 - way) * quarter, quarter)
-            shares[way, alone] = own_share_sum[alone].astype(bf16)
-            joined = own_share_sum[joint] + far_in[way, h].astype(f32)
-            shares[way, joint] = joined.astype(bf16)
+            alone, joint, cols = part(1 - way), part(way), side_cols(h)
+            shares[way, alone, cols] = own_share_sum[alone, cols].astype(bf16)
+            joined = own_share_sum[joint, cols] + far_in[way, h].astype(f32)
+            shares[way, joint, cols] = joined.astype(bf16)
             send_near(way, h).start()
     for cols, y in projected(tp):
         own_share_sum[:, cols] = y
     loads[1].wait()
 
-    def own_rows(h):
+    def own_cols(h):
         for way in range(2):
             send_near(way, h).wait_recv()
+        cols = side_cols(h)
         got = near_in[0, h].astype(f32) + near_in[1, h].astype(f32)
-        x = residual[part(h)].astype(f32) + (own_share_sum[part(h)] + got)
-        x = x.astype(bf16)
-        stream[part(h)] = x
-        x = x.astype(f32)
-        scale = lax.rsqrt(jnp.mean(x * x, axis=1, keepdims=True) + norm_eps)
-        normed[part(h)] = (x * scale * gain_ref[...]).astype(bf16)
+        x = residual[:, cols].astype(f32) + (own_share_sum[:, cols] + got)
+        stream[:, cols] = x.astype(bf16)
 
     ids = ids_ref[...]
     expert_at = lax.broadcasted_iota(jnp.int32, (ring * peers, rows), 0)
@@ -386,11 +391,12 @@
     def packing(n):
         return (chunk_row == places[n : n + 1, :]).astype(f32).astype(bf16)
 
-    def pack(n, way, entry):
+    def pack(n, way, entry, h):
         choose = packing(n)
-        for c in range(width // tile):
+        per_side = width // 2 // tile
+        for c in range(h * per_side, (h + 1) * per_side):
             cols = pl.ds(c * tile, tile)
-            got = jnp.dot(choose, normed[:, cols], preferred_element_type=f32)
+            got = jnp.dot(choose, stream[:, cols], preferred_element_type=f32)
             pool[way, entry, :, cols] = got.astype(bf16)
 
     def pack_meta(n, way, entry):
@@ -410,16 +416,13 @@
         pack_meta(n, way, FIRST[kind])
     pack_meta(5, 0, HOME)
 
-    own_rows(0)
-    own_rows(1)
-    for n, way, kind in packs:
-        pack(n, way, FIRST[kind])
-        if kind == 2:
-            for w in range(2):
-                forward(w, 2, 0, start_both)
-        else:
-            forward(way, kind, 0, start_both)
-    pack(5, 0, HOME)
+    for h in range(2):
+        own_cols(h)
+        for n, way, kind in packs:
+            pack(n, way, FIRST[kind], h)
+            for w in range(2) if kind == 2 else (way,):
+                forward(w, kind, 0, h, begin)
+        pack(5, 0, HOME, h)
 
     row_id = lax.broadcasted_iota(jnp.int32, (room, room), 0)
     local_code = (row_id // (2 * CAP)) * CAP + lax.rem(row_id, CAP)
@@ -469,12 +472,18 @@
     def pick(step):
         a, b = locate(paired(step)), locate(paired(ring - 1 - step))
         one_a, one_b = pick_of(*a, 0), pick_of(*b, 1)
+        square = jnp.zeros((room, 1), f32)
         for c in range(width // tile):
             cols = pl.ds(c * tile, tile)
             got = jnp.dot(one_a, pool[a[0], a[1], :, cols], preferred_element_type=f32)
             got += jnp.dot(one_b, pool[b[0], b[1], :, cols], preferred_element_type=f32)
-            got = got.astype(bf16).reshape(peers, 2 * CAP, tile)
-            picked[step, :, :, cols] = got
+            square += jnp.sum(got * got, axis=1, keepdims=True)
+            unscaled[:, cols] = got
+        scale = lax.rsqrt(square / width + norm_eps)
+        for c in range(width // tile):
+            cols = pl.ds(c * tile, tile)
+            got = (unscaled[:, cols] * scale * gain_ref[:, cols]).astype(bf16)
+            picked[step, :, :, cols] = got.reshape(peers, 2 * CAP, tile)
         for o in range(1, peers):
             exchange(picked, routed, pick_send, pick_recv, step, o).start()
         routed[step, mine] = picked[step, mine]
@@ -496,9 +505,10 @@
 
     def ring_step(d, _):
         for kind in (2, 1, 0):
-            for way in range(2):
-                receive(way, kind, d)
-                forward(way, kind, d, start_both)
+            for h in range(2):
+                for way in range(2):
+                    receive(way, kind, d, h)
+                    forward(way, kind, d, h, begin)
 
         @pl.when(d <= far - 1)
         def _():
@@ -657,7 +667,8 @@
     def drain(d, _):
         for kind in range(3):
             for way in range(2):
-                forward(way, kind, d, wait_sent)
+                for h in range(2):
+                    forward(way, kind, d, h, finish)
 
                 @pl.when(d >= 1)
                 def _():
@@ -689,7 +700,7 @@
     peers = xs * CORES
     hidden = gate.shape[1]
     room = 2 * peers * CAP
-    tile = min(512, width)
+    tile = min(512, width // 2)
     bf16, f32 = jnp.bfloat16, jnp.float32
     vmem = pl.BlockSpec(memory_space=pltpu.VMEM)
     smem = pl.BlockSpec(memory_space=pltpu.SMEM)
@@ -707,11 +718,11 @@
             pltpu.VMEM((rows, width), bf16),
             pltpu.VMEM(proj.shape, bf16),
             pltpu.VMEM((3, rows, width), bf16),
-            pltpu.VMEM((2, 2, rows // 4, width), bf16),
-            pltpu.VMEM((2, 2, rows // 2, width), bf16),
+            pltpu.VMEM((2, 2, rows // 2, width // 2), bf16),
+            pltpu.VMEM((2, 2, rows, width // 2), bf16),
             pltpu.VMEM((rows, width), f32),
             pltpu.VMEM((rows, width), bf16),
-            pltpu.VMEM((rows, width), bf16),
+            pltpu.VMEM((room, width), f32),
             pltpu.VMEM((8, rows), f32),
             pltpu.VMEM((2, ENTRIES, room, width), bf16),
             pltpu.VMEM((rows, width), f32),
@@ -726,8 +737,8 @@
             pltpu.VMEM((width, hidden), bf16),
             pltpu.VMEM((hidden, width), bf16),
             dma((5,)),
-            dma((2, ENTRIES)),
-            dma((2, ENTRIES)),
+            dma((2, ENTRIES, 2)),
+            dma((2, ENTRIES, 2)),
             dma((2, ENTRIES)),
             dma((2, ENTRIES)),
             dma((far, peers)),

time: 212 us -> 208 us (0.981)
  Pallas kernels: 209 us -> 205 us
    pallas_call x1, Pallas kernels: 209 us -> 205 us  [layer(): pl.pallas_call(functools.partial(expert_kernel, ring, xs, tile), out_shap...]
where the time goes in v8:
time: 208 us
  Pallas kernels  205 us (99%)
    pallas_call x1, Pallas kernels, layer(): pl.pallas_call(functools.partial(expert_kernel, ring, xs, tile), out_shap...  205 us

profile of v8, /device:TPU:40, one launch (start us, length us, event | category | flops | bytes accessed | tf_op | source)
XLA Modules:
  0.0 207.7 jit_solution(16194883684065361172)
XLA Ops:
  0.0 1.0 multiply_sine_fusion
  1.0 204.8 %shard_map.118 = bf16[128,2048]{1,0:T(8,128)(2,1)} custom-call(bf16[512,256]{1,0:T(8,128)(2,1)} %query_ref.1, bf16[64,512]{1,0:T(8,128)(2,1)} %bitcast.11, bf16[64,512]{1,0:T(8,128)(2,1)} %bitcast.12, f32[32,512]{1,0:T(8,128)} %get-tuple-element.6.cos_ref, f32[32,512]{1,0:T(8,128)} %get-tuple-element.5.sin_ref, f32[4]{0:T(128)} %sink_ref.1, ...), custom_call_target="tpu_custom_call" | custom-call | tf_op jit(solution)/shard_map/pallas_call | solution.py:710
  205.8 1.9 copy.14
  (2 shorter events, 0.0 us)

commit v9 on v8

--- a/solution.py
+++ b/solution.py
@@ -96,6 +96,8 @@
     nxt = {"sp": lax.rem(sp + CORES, ring * CORES)}
     prv = {"sp": lax.rem(sp + (ring - 1) * CORES, ring * CORES)}
 
+    far_first = sorted(range(1, peers), key=lambda o: -min(o % xs, xs - o % xs))
+
     def peer(offset):
         u = lax.rem(mine + offset, peers)
         return u, {"sp": z * CORES + u // xs, "tp": lax.rem(u, xs)}
@@ -313,21 +315,23 @@
         )
 
     loads[0].wait()
-    for cols, y in projected(lax.rem(tp + 2, xs)):
+    per_side = width // 2 // tile
+    for c, (cols, y) in enumerate(projected(lax.rem(tp + 2, xs))):
         shares[2, :, cols] = y.astype(bf16)
-    for h in range(2):
-        for way in range(2):
-            send_far(way, h).start()
+        if (c + 1) % per_side == 0:
+            for way in range(2):
+                send_far(way, c // per_side).start()
     for way in range(2):
-        for cols, y in projected(lax.rem(tp + 1 - 2 * way + xs, xs)):
+        for c, (cols, y) in enumerate(projected(lax.rem(tp + 1 - 2 * way + xs, xs))):
             own_share_sum[:, cols] = y
-        for h in range(2):
-            send_far(way, h).wait_recv()
-            alone, joint, cols = part(1 - way), part(way), side_cols(h)
-            shares[way, alone, cols] = own_share_sum[alone, cols].astype(bf16)
-            joined = own_share_sum[joint, cols] + far_in[way, h].astype(f32)
-            shares[way, joint, cols] = joined.astype(bf16)
-            send_near(way, h).start()
+            if (c + 1) % per_side == 0:
+                h = c // per_side
+                send_far(way, h).wait_recv()
+                alone, joint, side = part(1 - way), part(way), side_cols(h)
+                shares[way, alone, side] = own_share_sum[alone, side].astype(bf16)
+                joined = own_share_sum[joint, side] + far_in[way, h].astype(f32)
+                shares[way, joint, side] = joined.astype(bf16)
+                send_near(way, h).start()
     for cols, y in projected(tp):
         own_share_sum[:, cols] = y
     loads[1].wait()
@@ -393,7 +397,6 @@
 
     def pack(n, way, entry, h):
         choose = packing(n)
-        per_side = width // 2 // tile
         for c in range(h * per_side, (h + 1) * per_side):
             cols = pl.ds(c * tile, tile)
             got = jnp.dot(choose, stream[:, cols], preferred_element_type=f32)
@@ -484,7 +487,7 @@
             cols = pl.ds(c * tile, tile)
             got = (unscaled[:, cols] * scale * gain_ref[:, cols]).astype(bf16)
             picked[step, :, :, cols] = got.reshape(peers, 2 * CAP, tile)
-        for o in range(1, peers):
+        for o in far_first:
             exchange(picked, routed, pick_send, pick_recv, step, o).start()
         routed[step, mine] = picked[step, mine]
 
@@ -499,7 +502,7 @@
             cols = pl.ds(c * tile, tile)
             y = jnp.dot(hidden, down_w[:, cols], preferred_element_type=f32)
             made[step, :, :, cols] = y.astype(bf16).reshape(peers, 2 * CAP, tile)
-        for o in range(1, peers):
+        for o in far_first:
             exchange(made, back, back_send, back_recv, step, o).start()
         back[step, mine] = made[step, mine]
 

time: 208 us -> 206 us (level)
  Pallas kernels: 205 us -> 202 us
    pallas_call x1, Pallas kernels: 205 us -> 202 us  [layer(): pl.pallas_call(functools.partial(expert_kernel, ring, xs, tile), out_shap...]
where the time goes in v9:
time: 206 us; the launch traced here: 205 us
  Pallas kernels  202 us (98%)
    pallas_call x1, Pallas kernels, layer(): pl.pallas_call(functools.partial(expert_kernel, ring, xs, tile), out_shap...  202 us

profile of v9, /device:TPU:40, one launch (start us, length us, event | category | flops | bytes accessed | tf_op | source)
XLA Modules:
  0.0 205.3 jit_solution(5745770371148252875)
XLA Ops:
  0.0 1.0 multiply_sine_fusion
  1.0 202.5 %shard_map.118 = bf16[128,2048]{1,0:T(8,128)(2,1)} custom-call(bf16[512,256]{1,0:T(8,128)(2,1)} %query_ref.1, bf16[64,512]{1,0:T(8,128)(2,1)} %bitcast.11, bf16[64,512]{1,0:T(8,128)(2,1)} %bitcast.12, f32[32,512]{1,0:T(8,128)} %get-tuple-element.6.cos_ref, f32[32,512]{1,0:T(8,128)} %get-tuple-element.5.sin_ref, f32[4]{0:T(128)} %sink_ref.1, ...), custom_call_target="tpu_custom_call" | custom-call | tf_op jit(solution)/shard_map/pallas_call | solution.py:713
  203.5 1.9 copy.14
  (2 shorter events, 0.0 us)

commit v10 on v9

--- a/solution.py
+++ b/solution.py
@@ -162,7 +162,6 @@
     for c in range(query_ref.shape[1] // 128):
         cols = pl.ds(c * 128, 128)
         rot_q[:, cols] = rotated(query_ref[:, cols], cosines, sines)
-    halo.wait_recv()
 
     def part(h):
         return pl.ds(h * half, half)
@@ -267,8 +266,13 @@
     k_at = lax.broadcasted_iota(jnp.int32, (WINDOW, 2 * WINDOW), 1)
     reach = q_at + WINDOW - k_at
 
-    def projected(block):
-        start = pl.multiple_of(block * WINDOW, WINDOW)
+    def projected(rank):
+
+        @pl.when(rank == 0)
+        def _():
+            halo.wait_recv()
+
+        start = pl.multiple_of(rank * WINDOW, WINDOW)
         first = start + sp * tok
         allowed = (reach >= 0) & (reach < WINDOW) & (k_at + first >= WINDOW)
         k = keys_values[0:HDIM, pl.ds(start, 2 * WINDOW)]

time: 206 us -> 206 us (level)
  no operation moved by 1% of the time
where the time goes in v10:
time: 206 us
  Pallas kernels  203 us (99%)
    pallas_call x1, Pallas kernels, layer(): pl.pallas_call(functools.partial(expert_kernel, ring, xs, tile), out_shap...  203 us

profile of v10, /device:TPU:40, one launch (start us, length us, event | category | flops | bytes accessed | tf_op | source)
XLA Modules:
  0.0 205.7 jit_solution(17185966423406106948)
XLA Ops:
  0.0 1.0 multiply_sine_fusion
  1.0 202.8 %shard_map.118 = bf16[128,2048]{1,0:T(8,128)(2,1)} custom-call(bf16[512,256]{1,0:T(8,128)(2,1)} %query_ref.1, bf16[64,512]{1,0:T(8,128)(2,1)} %bitcast.11, bf16[64,512]{1,0:T(8,128)(2,1)} %bitcast.12, f32[32,512]{1,0:T(8,128)} %get-tuple-element.6.cos_ref, f32[32,512]{1,0:T(8,128)} %get-tuple-element.5.sin_ref, f32[4]{0:T(128)} %sink_ref.1, ...), custom_call_target="tpu_custom_call" | custom-call | tf_op jit(solution)/shard_map/pallas_call | solution.py:717
  203.8 1.9 copy.14
  (2 shorter events, 0.0 us)
